TPU v7x, 256 devices: a 2x2x32 block of a 4x16x32 slice. The times are simulated.
256 devices in a mesh: grp: 4 (over y, x), ep: 32 (over z), tp: 2 (over core).
Axes of the slice: x: 2, y: 2, z: 32, core: 2. Of those that a mesh axis runs over, the one named last changes fastest.
The devices are a block of a 4x16x32 slice.
Arguments:
- tokens: bfloat16 [4096, 2048], P(('grp', 'ep')), parts along dimension 0, may hold values from -6 to 6
- norm_gain: float32 [2048], replicated, may hold values from 0.1 to 1.9
- group_prob: float32 [4096], P(('grp', 'ep')), parts along dimension 0, may hold values from 0.5 to 1
- route_logits: float32 [4096, 4], P(('grp', 'ep')), parts along dimension 0, may hold values from -6 to 6
- expert_ids: int32 [4096, 4], P(('grp', 'ep')), parts along dimension 0, may hold values from 0 to 31, as said below
- w_gate: bfloat16 [32, 2048, 512], P('ep', None, 'tp'), may hold values from -0.125 to 0.125
- w_up: bfloat16 [32, 2048, 512], P('ep', None, 'tp'), may hold values from -0.125 to 0.125
- w_down: bfloat16 [32, 512, 2048], P('ep', 'tp'), may hold values from -0.25 to 0.25
Outputs:
- mixed: bfloat16 [4096, 2048], P(('grp', 'ep')), parts along dimension 0
There are 4 independent parts, one for each index of `grp`. A program takes and returns all parts, laid end to end along the dimension named above; an argument that names none is the same for every part. Nothing has to cross between parts.
Inputs may be any that keep to these rules, and one draw needn't show every extreme that they name: `expert_ids`: each token names 4 different experts, all inside one group of 16 consecutive experts. Of the 32 tokens of one index of ep, exactly 16 lie in each group, so at most 16 of them name any one expert; in every draw some expert is named by 16 tokens of every index of ep.
All inputs are finite; a program needn't handle non-finite values.
Results may differ from a plain program's by a relative error of at most 0.0077.
Values may be sent and summed in bfloat16 or wider, within the bound.
No kernel may reach another device: no remote copies, remote signals or barrier semaphores. Data moves between devices by JAX's collectives and lax.ppermute only.
A program may use at most 64 MiB of HBM per device.

v0:
```python
import functools

import jax
import jax.numpy as jnp
from jax import lax
from jax.experimental import pallas as pl
from jax.experimental.pallas import tpu as pltpu
from jax.sharding import PartitionSpec as P


LANES = 128
STEPS = 4
GATHER = (0, 1, 0, 3, 4, 0, 6, 6, 8, 6, 10, 11, 10, 13, 13, 15)
GATHER_ORDER = (6, 1, 3, 10, 8, 4, 7, 13, 11, 5, 2, 15, 14, 12, 9, 16)
COMBINE = (0, 1, 1, 3, 0, 5, 6, 6, 8, 5, 10, 11, 11, 10, 14, 14)
COMBINE_ORDER = (16, 15, 13, 12, 9, 14, 11, 4, 7, 8, 10, 6, 2, 3, 5, 1)
LAST = len(GATHER)


def prepare_kernel(tokens, gain, prob, logits, ids, unit, kept):
    rows, width = unit.shape
    model = tokens.shape[1]
    values = tokens[...].astype(jnp.float32)
    scale = lax.rsqrt(jnp.mean(values * values, axis=-1, keepdims=True) + 1e-06)
    unit[:, :model] = (values * scale * gain[...]).astype(jnp.bfloat16)
    expw = jnp.exp(logits[...])
    route_w = prob[...] * expw / jnp.sum(expw, axis=0, keepdims=True)
    picks, count = expw.shape
    experts = lax.axis_size("ep")
    expert = lax.broadcasted_iota(jnp.int32, (experts, count), 0)
    dense = jnp.zeros((experts, count), jnp.float32)
    for k in range(picks):
        dense += jnp.where(ids[k : k + 1, :] == expert, route_w[k : k + 1, :], 0.0)
    high = dense.astype(jnp.bfloat16).astype(jnp.float32)
    low = dense - high
    table = jnp.concatenate(
        [high, low, jnp.zeros((width - model - 2 * experts, count), jnp.float32)], axis=0
    ).astype(jnp.bfloat16)
    row = lax.broadcasted_iota(jnp.int32, (rows, count), 0)
    chosen = (lax.broadcasted_iota(jnp.int32, (rows, count), 1) == row).astype(jnp.bfloat16)
    unit[:, model:] = lax.dot_general(
        chosen, table, (((1,), (1,)), ((), ())), preferred_element_type=jnp.float32
    ).astype(jnp.bfloat16)
    kept[...] = unit[...]


def pieces(n, rows, core):
    half, at = rows // 2, 0
    mine = pl.ds(pl.multiple_of(core * half, half), half)
    for k in range(n):
        some, count = (mine, half) if k in (0, n - 1) else (slice(None), rows)
        yield k, some, slice(at, at + count)
        at += count


def block(x, gate_w, up_w, down_w):
    gate = jnp.dot(x, gate_w[0], preferred_element_type=jnp.float32)
    up = jnp.dot(x, up_w[0], preferred_element_type=jnp.float32)
    act = (gate / (1.0 + jnp.exp(-gate)) * up).astype(jnp.bfloat16)
    return jnp.dot(act, down_w[0], preferred_element_type=jnp.float32).astype(jnp.bfloat16)


def chunks(total, body):
    step = total // STEPS

    def one(i, carry):
        body(pl.ds(pl.multiple_of(i * step, step), step))
        return carry

    lax.fori_loop(0, STEPS, one, 0)


def first_kernel(n, *refs):
    units, other, (rows_all, weight_all, part_all) = refs[:n], refs[n : n + 3], refs[n + 3 :]
    rows, _ = units[0].shape
    total_rows, model = rows_all.shape
    me, core = lax.axis_index("ep"), lax.axis_index("tp")
    experts = lax.axis_size("ep")
    for k, some, at in pieces(n, rows, core):
        rows_all[at, :] = units[k][some, :model]
        table = units[k][some, model:].astype(jnp.float32)
        lane = lax.broadcasted_iota(jnp.int32, table.shape, 1)
        taken = jnp.where((lane == me) | (lane == me + experts), table, 0.0)
        weight_all[at, :] = jnp.broadcast_to(jnp.sum(taken, axis=1, keepdims=True), table.shape)

    def body(at):
        part_all[at, :] = block(rows_all[at, :], *other)

    chunks(total_rows, body)


def second_kernel(n, *refs):
    (rows_all, weight_all, part_all, *own), outs, mixed_all = refs[:6], refs[6 : 6 + n], refs[-1]

    def body(at):
        part = block(rows_all[at, :], *own).astype(jnp.float32)
        total = (part_all[at, :].astype(jnp.float32) + part).astype(jnp.bfloat16)
        weighted = total.astype(jnp.float32) * weight_all[at, :1]
        mixed_all[at, :] = weighted.astype(jnp.bfloat16)

    chunks(rows_all.shape[0], body)
    for k, some, at in pieces(n, outs[0].shape[0], lax.axis_index("tp")):
        if k in (0, n - 1):
            outs[k][...] = jnp.zeros_like(outs[k])
        outs[k][some, :] = mixed_all[at, :]


VMEM = pl.BlockSpec(memory_space=pltpu.VMEM)


def prepare(tokens, norm_gain, group_prob, route_logits, expert_ids):
    rows, model = tokens.shape
    return pl.pallas_call(
        prepare_kernel,
        out_shape=[jax.ShapeDtypeStruct((rows, model + LANES), jnp.bfloat16)] * 2,
        in_specs=[VMEM] * 5,
        out_specs=[VMEM] * 2,
        name="prepare",
    )(tokens, norm_gain[None, :], group_prob[None, :], route_logits.T, expert_ids.T)


def expert(units, own, other):
    n = len(units)
    rows, width = units[0].shape
    model = width - LANES
    total = (n - 1) * rows
    params = pltpu.CompilerParams(vmem_limit_bytes=20 * 1024 * 1024)
    whole = jax.ShapeDtypeStruct((total, model), jnp.bfloat16)
    held = pl.pallas_call(
        functools.partial(first_kernel, n),
        out_shape=[whole, jax.ShapeDtypeStruct((total, LANES), jnp.float32), whole],
        in_specs=[VMEM] * (n + 3),
        out_specs=[VMEM] * 3,
        compiler_params=params,
        name="first",
    )(*units, *other)
    return pl.pallas_call(
        functools.partial(second_kernel, n),
        out_shape=[jax.ShapeDtypeStruct((rows, model), jnp.bfloat16)] * n,
        in_specs=[VMEM] * 6,
        out_specs=[VMEM] * n,
        scratch_shapes=[pltpu.VMEM((total, model), jnp.bfloat16)],
        compiler_params=params,
        name="second",
    )(*held, *own)


def turned(array, shift):
    n, cores = lax.axis_size("ep"), lax.axis_size("tp")
    pairs = []
    for i in range(n):
        for core in range(cores):
            to = (i + (shift if core == 0 else -shift)) % n
            pairs.append((i * cores + core, to * cores + core))
    return lax.ppermute(array, ("ep", "tp"), pairs)


def swapped(array):
    return lax.ppermute(array, "tp", [(0, 1), (1, 0)])


def added(*parts):
    total = parts[0].astype(jnp.float32)
    for part in parts[1:]:
        total = total + part.astype(jnp.float32)
    return total.astype(jnp.bfloat16)


def gather(unit):
    held = {0: unit}
    for at in GATHER_ORDER:
        held[at] = turned(held[GATHER[at - 1]], at - GATHER[at - 1])
    return [held[at] for at in range(LAST + 1)]


def combine(outs):
    parts = {at: [out] for at, out in enumerate(outs)}
    for at in COMBINE_ORDER:
        whole = added(*parts[at]) if len(parts[at]) > 1 else outs[at]
        parts[COMBINE[at - 1]].append(turned(whole, COMBINE[at - 1] - at))
    return added(*parts[0])


def shards(tokens, norm_gain, group_prob, route_logits, expert_ids, w_gate, w_up, w_down):
    own, other = (w_gate, w_up, w_down), []
    for w in own:
        other.append(swapped(w))
    unit, kept = prepare(tokens, norm_gain, group_prob, route_logits, expert_ids)
    units = gather(unit)
    mixed = combine(expert([kept, *units[1:]], own, other))
    return added(mixed, swapped(mixed))


def solution(mesh):
    in_specs = (
        P(("grp", "ep"), None),
        P(),
        P(("grp", "ep")),
        P(("grp", "ep"), None),
        P(("grp", "ep"), None),
        P("ep", None, "tp"),
        P("ep", None, "tp"),
        P("ep", "tp", None),
    )
    out_specs = P(("grp", "ep"), None)
    return jax.shard_map(
        shards, mesh=mesh, in_specs=in_specs, out_specs=out_specs, check_vma=False
    )
```

profile of v0, /device:TPU:38, one launch (start us, length us, event | category | flops | bytes accessed | tf_op | source)
XLA Modules:
  0.0 160.2 jit_solution(16347013861333225968)
XLA Ops:
  1.8 11.1 %collective-permute-start.5 = (bf16[32,2176]{1,0:T(8,128)(2,1)}, bf16[32,2176]{1,0:T(8,128)(2,1)S(1)}, u32[]{:S(2)}, u32[]{:S(2)}) collective-permute-start(bf16[32,2176]{1,0:T(8,128)(2,1)} %get-tuple-element.28), channel_id=1, source_target_pairs={{0,12},{1,53},{2,14},{3,55},{4,16},{5,57},{6,18},{7,59},{8,20},{9,... | collective-permute-start | bytes 417800 | tf_op jit(solution)/shard_map/ppermute | solution.py:155
  12.9 6.4 %collective-permute-start.2 = (bf16[32,2176]{1,0:T(8,128)(2,1)}, bf16[32,2176]{1,0:T(8,128)(2,1)S(1)}, u32[]{:S(2)}, u32[]{:S(2)}) collective-permute-start(bf16[32,2176]{1,0:T(8,128)(2,1)} %get-tuple-element.28), channel_id=1, source_target_pairs={{0,6},{1,59},{2,8},{3,61},{4,10},{5,63},{6,12},{7,1},{8,14},{9,3},... | collective-permute-start | bytes 417800 | tf_op jit(solution)/shard_map/ppermute | solution.py:155
  19.4 9.7 %collective-permute-start.16 = (bf16[1,2048,256]{2,1,0:T(8,128)(2,1)}, bf16[1,2048,256]{2,1,0:T(8,128)(2,1)S(1)}, u32[]{:S(2)}, u32[]{:S(2)}) collective-permute-start(bf16[1,2048,256]{2,1,0:T(8,128)(2,1)} %refs_3_.1), channel_id=1, source_target_pairs={{0,1},{1,0},{2,3},{3,2},{4,5},{5,4},{6,7},{7,6},{8,9},{9,8},{10,11... | collective-permute-start | bytes 3145736 | tf_op jit(solution)/shard_map/ppermute | solution.py:159
  31.0 4.1 %collective-permute-start = (bf16[32,2176]{1,0:T(8,128)(2,1)}, bf16[32,2176]{1,0:T(8,128)(2,1)S(1)}, u32[]{:S(2)}, u32[]{:S(2)}) collective-permute-start(bf16[32,2176]{1,0:T(8,128)(2,1)} %get-tuple-element.28), channel_id=1, source_target_pairs={{0,2},{1,63},{2,4},{3,1},{4,6},{5,3},{6,8},{7,5},{8,10},{9,7},{10,... | collective-permute-start | bytes 417800 | tf_op jit(solution)/shard_map/ppermute | solution.py:155
  35.1 4.6 %collective-permute-done.2.refs_3_ = bf16[32,2176]{1,0:T(8,128)(2,1)S(1)} collective-permute-done((bf16[32,2176]{1,0:T(8,128)(2,1)}, bf16[32,2176]{1,0:T(8,128)(2,1)S(1)}, u32[]{:S(2)}, u32[]{:S(2)}) %collective-permute-start.2) | collective-permute-done | bytes 139296 | tf_op jit(solution)/shard_map/ppermute | solution.py:155
  39.7 4.9 %collective-permute-start.9 = (bf16[32,2176]{1,0:T(8,128)(2,1)S(1)}, bf16[32,2176]{1,0:T(8,128)(2,1)S(1)}, u32[]{:S(2)}, u32[]{:S(2)}) collective-permute-start(bf16[32,2176]{1,0:T(8,128)(2,1)S(1)} %collective-permute-done.5.refs_6_), channel_id=1, source_target_pairs={{0,8},{1,57},{2,10},{3,59},{4,12},{5,61},{6,14},{7,63},{8,16},{9,1... | collective-permute-start | bytes 417800 | tf_op jit(solution)/shard_map/ppermute | solution.py:155
  44.7 6.7 %collective-permute-done.refs_1_ = bf16[32,2176]{1,0:T(8,128)(2,1)S(1)} collective-permute-done((bf16[32,2176]{1,0:T(8,128)(2,1)}, bf16[32,2176]{1,0:T(8,128)(2,1)S(1)}, u32[]{:S(2)}, u32[]{:S(2)}) %collective-permute-start) | collective-permute-done | bytes 139296 | tf_op jit(solution)/shard_map/ppermute | solution.py:155
  51.4 8.5 %collective-permute-done.7.refs_8_ = bf16[32,2176]{1,0:T(8,128)(2,1)S(1)} collective-permute-done((bf16[32,2176]{1,0:T(8,128)(2,1)S(1)}, bf16[32,2176]{1,0:T(8,128)(2,1)S(1)}, u32[]{:S(2)}, u32[]{:S(2)}) %collective-permute-start.7) | collective-permute-done | bytes 139296 | tf_op jit(solution)/shard_map/ppermute | solution.py:155
  60.3 5.8 %collective-permute-done.3.refs_4_ = bf16[32,2176]{1,0:T(8,128)(2,1)S(1)} collective-permute-done((bf16[32,2176]{1,0:T(8,128)(2,1)S(1)}, bf16[32,2176]{1,0:T(8,128)(2,1)S(1)}, u32[]{:S(2)}, u32[]{:S(2)}) %collective-permute-start.3) | collective-permute-done | bytes 139296 | tf_op jit(solution)/shard_map/ppermute | solution.py:155
  67.6 7.4 %collective-permute-done.12.refs_13_ = bf16[32,2176]{1,0:T(8,128)(2,1)S(1)} collective-permute-done((bf16[32,2176]{1,0:T(8,128)(2,1)S(1)}, bf16[32,2176]{1,0:T(8,128)(2,1)S(1)}, u32[]{:S(2)}, u32[]{:S(2)}) %collective-permute-start.12) | collective-permute-done | bytes 139296 | tf_op jit(solution)/shard_map/ppermute | solution.py:155
  76.0 5.3 %collective-permute-done.8.refs_9_ = bf16[32,2176]{1,0:T(8,128)(2,1)S(1)} collective-permute-done((bf16[32,2176]{1,0:T(8,128)(2,1)S(1)}, bf16[32,2176]{1,0:T(8,128)(2,1)S(1)}, u32[]{:S(2)}, u32[]{:S(2)}) %collective-permute-start.8) | collective-permute-done | bytes 139296 | tf_op jit(solution)/shard_map/ppermute | solution.py:155
  82.8 5.8 %collective-permute-done.14.refs_15_ = bf16[32,2176]{1,0:T(8,128)(2,1)S(1)} collective-permute-done((bf16[32,2176]{1,0:T(8,128)(2,1)S(1)}, bf16[32,2176]{1,0:T(8,128)(2,1)S(1)}, u32[]{:S(2)}, u32[]{:S(2)}) %collective-permute-start.14) | collective-permute-done | bytes 139296 | tf_op jit(solution)/shard_map/ppermute | solution.py:155
  90.0 4.9 %collective-permute-done.11.refs_12_ = bf16[32,2176]{1,0:T(8,128)(2,1)S(1)} collective-permute-done((bf16[32,2176]{1,0:T(8,128)(2,1)S(1)}, bf16[32,2176]{1,0:T(8,128)(2,1)S(1)}, u32[]{:S(2)}, u32[]{:S(2)}) %collective-permute-start.11) | collective-permute-done | bytes 139296 | tf_op jit(solution)/shard_map/ppermute | solution.py:155
  97.3 3.1 %first.1 = (bf16[512,2048]{1,0:T(8,128)(2,1)S(1)}, f32[512,128]{1,0:T(8,128)S(1)}, bf16[512,2048]{1,0:T(8,128)(2,1)S(1)}) custom-call(bf16[32,2176]{1,0:T(8,128)(2,1)S(1)} %copy-done.3, bf16[32,2176]{1,0:T(8,128)(2,1)S(1)} %collective-permute-done.refs_1_, bf16[32,2176]{1,0:T(8,128)(2,1)S(1)} %collective-permute-done.1.refs_2_, ...), custom_call_target="tpu_custom_call" | custom-call | tf_op jit(solution)/shard_map/first/pallas_call | solution.py:129
  100.4 3.4 %second.1 = (bf16[32,2048]{1,0:T(8,128)(2,1)S(1)}, bf16[32,2048]{1,0:T(8,128)(2,1)S(1)}, bf16[32,2048]{1,0:T(8,128)(2,1)S(1)}, bf16[32,2048]{1,0:T(8,128)(2,1)S(...) custom-call(bf16[512,2048]{1,0:T(8,128)(2,1)S(1)} %get-tuple-element, ...), custom_call_target="tpu_custom_call" | custom-call | tf_op jit(solution)/shard_map/second/pallas_call | solution.py:137
  104.7 3.2 %collective-permute-start.22 = (bf16[32,2048]{1,0:T(8,128)(2,1)S(1)}, bf16[32,2048]{1,0:T(8,128)(2,1)S(1)}, u32[]{:S(2)}, u32[]{:S(2)}) collective-permute-start(bf16[32,2048]{1,0:T(8,128)(2,1)S(1)} %get-tuple-element.39), channel_id=1, source_target_pairs={{0,60},{1,5},{2,62},{3,7},{4,0},{5,9},{6,2},{7,11},{8,4},{9,13},{1... | collective-permute-start | bytes 393224 | tf_op jit(solution)/shard_map/ppermute | solution.py:155
  109.9 3.1 %collective-permute-start.27 = (bf16[32,2048]{1,0:T(8,128)(2,1)S(1)}, bf16[32,2048]{1,0:T(8,128)(2,1)S(1)}, u32[]{:S(2)}, u32[]{:S(2)}) collective-permute-start(bf16[32,2048]{1,0:T(8,128)(2,1)S(1)} %get-tuple-element.44), channel_id=1, source_target_pairs={{0,62},{1,3},{2,0},{3,5},{4,2},{5,7},{6,4},{7,9},{8,6},{9,11},{10,... | collective-permute-start | bytes 393224 | tf_op jit(solution)/shard_map/ppermute | solution.py:155
  114.0 3.2 %collective-permute-start.32 = (bf16[32,2048]{1,0:T(8,128)(2,1)S(1)}, bf16[32,2048]{1,0:T(8,128)(2,1)S(1)}, u32[]{:S(2)}, u32[]{:S(2)}) collective-permute-start(bf16[32,2048]{1,0:T(8,128)(2,1)S(1)} %get-tuple-element.48), channel_id=1, source_target_pairs={{0,62},{1,3},{2,0},{3,5},{4,2},{5,7},{6,4},{7,9},{8,6},{9,11},{10,... | collective-permute-start | bytes 393224 | tf_op jit(solution)/shard_map/ppermute | solution.py:155
  117.2 2.9 %collective-permute-start.21 = (bf16[32,2048]{1,0:T(8,128)(2,1)S(1)}, bf16[32,2048]{1,0:T(8,128)(2,1)S(1)}, u32[]{:S(2)}, u32[]{:S(2)}) collective-permute-start(bf16[32,2048]{1,0:T(8,128)(2,1)S(1)} %add_convert_fusion.9), channel_id=1, source_target_pairs={{0,56},{1,9},{2,58},{3,11},{4,60},{5,13},{6,62},{7,15},{8,0},{9,17... | collective-permute-start | bytes 393224 | tf_op jit(solution)/shard_map/ppermute | solution.py:155
  122.3 6.8 %collective-permute-done.21 = bf16[32,2048]{1,0:T(8,128)(2,1)S(1)} collective-permute-done((bf16[32,2048]{1,0:T(8,128)(2,1)S(1)}, bf16[32,2048]{1,0:T(8,128)(2,1)S(1)}, u32[]{:S(2)}, u32[]{:S(2)}) %collective-permute-start.21) | collective-permute-done | bytes 131104 | tf_op jit(solution)/shard_map/ppermute | solution.py:155
  129.2 4.9 %collective-permute-start.25 = (bf16[32,2048]{1,0:T(8,128)(2,1)S(1)}, bf16[32,2048]{1,0:T(8,128)(2,1)S(1)}, u32[]{:S(2)}, u32[]{:S(2)}) collective-permute-start(bf16[32,2048]{1,0:T(8,128)(2,1)S(1)} %add_convert_fusion.7), channel_id=1, source_target_pairs={{0,54},{1,11},{2,56},{3,13},{4,58},{5,15},{6,60},{7,17},{8,62},{9,... | collective-permute-start | bytes 393224 | tf_op jit(solution)/shard_map/ppermute | solution.py:155
  136.6 5.6 %collective-permute-done.25 = bf16[32,2048]{1,0:T(8,128)(2,1)S(1)} collective-permute-done((bf16[32,2048]{1,0:T(8,128)(2,1)S(1)}, bf16[32,2048]{1,0:T(8,128)(2,1)S(1)}, u32[]{:S(2)}, u32[]{:S(2)}) %collective-permute-start.25) | collective-permute-done | bytes 131104 | tf_op jit(solution)/shard_map/ppermute | solution.py:155
  142.2 7.8 %collective-permute-start.30 = (bf16[32,2048]{1,0:T(8,128)(2,1)S(1)}, bf16[32,2048]{1,0:T(8,128)(2,1)S(1)}, u32[]{:S(2)}, u32[]{:S(2)}) collective-permute-start(bf16[32,2048]{1,0:T(8,128)(2,1)S(1)} %add_convert_fusion.4), channel_id=1, source_target_pairs={{0,54},{1,11},{2,56},{3,13},{4,58},{5,15},{6,60},{7,17},{8,62},{9,... | collective-permute-start | bytes 393224 | tf_op jit(solution)/shard_map/ppermute | solution.py:155
  150.0 8.0 %collective-permute-done.30 = bf16[32,2048]{1,0:T(8,128)(2,1)S(1)} collective-permute-done((bf16[32,2048]{1,0:T(8,128)(2,1)S(1)}, bf16[32,2048]{1,0:T(8,128)(2,1)S(1)}, u32[]{:S(2)}, u32[]{:S(2)}) %collective-permute-start.30) | collective-permute-done | bytes 131104 | tf_op jit(solution)/shard_map/ppermute | solution.py:155
  (69 shorter events, 22.8 us)
Async XLA Ops:
  1.8 29.2 %collective-permute-start.5 = (bf16[32,2176]{1,0:T(8,128)(2,1)}, bf16[32,2176]{1,0:T(8,128)(2,1)S(1)}, u32[]{:S(2)}, u32[]{:S(2)}) collective-permute-start(bf16[32,2176]{1,0:T(8,128)(2,1)} %get-tuple-element.28), channel_id=1, source_target_pairs={{0,12},{1,53},{2,14},{3,55},{4,16},{5,57},{6,18},{7,59},{8,20},{9,... | collective-permute-start | bytes 417800 | tf_op jit(solution)/shard_map/ppermute | solution.py:155
  12.9 26.8 %collective-permute-start.2 = (bf16[32,2176]{1,0:T(8,128)(2,1)}, bf16[32,2176]{1,0:T(8,128)(2,1)S(1)}, u32[]{:S(2)}, u32[]{:S(2)}) collective-permute-start(bf16[32,2176]{1,0:T(8,128)(2,1)} %get-tuple-element.28), channel_id=1, source_target_pairs={{0,6},{1,59},{2,8},{3,61},{4,10},{5,63},{6,12},{7,1},{8,14},{9,3},... | collective-permute-start | bytes 417800 | tf_op jit(solution)/shard_map/ppermute | solution.py:155
  19.4 77.0 %collective-permute-start.16 = (bf16[1,2048,256]{2,1,0:T(8,128)(2,1)}, bf16[1,2048,256]{2,1,0:T(8,128)(2,1)S(1)}, u32[]{:S(2)}, u32[]{:S(2)}) collective-permute-start(bf16[1,2048,256]{2,1,0:T(8,128)(2,1)} %refs_3_.1), channel_id=1, source_target_pairs={{0,1},{1,0},{2,3},{3,2},{4,5},{5,4},{6,7},{7,6},{8,9},{9,8},{10,11... | collective-permute-start | bytes 3145736 | tf_op jit(solution)/shard_map/ppermute | solution.py:159
  29.1 67.2 %collective-permute-start.17 = (bf16[1,2048,256]{2,1,0:T(8,128)(2,1)}, bf16[1,2048,256]{2,1,0:T(8,128)(2,1)S(1)}, u32[]{:S(2)}, u32[]{:S(2)}) collective-permute-start(bf16[1,2048,256]{2,1,0:T(8,128)(2,1)} %refs_4_.1), channel_id=1, source_target_pairs={{0,1},{1,0},{2,3},{3,2},{4,5},{5,4},{6,7},{7,6},{8,9},{9,8},{10,11... | collective-permute-start | bytes 3145736 | tf_op jit(solution)/shard_map/ppermute | solution.py:159
  29.1 67.2 %collective-permute-start.18 = (bf16[1,256,2048]{2,1,0:T(8,128)(2,1)}, bf16[1,256,2048]{2,1,0:T(8,128)(2,1)S(1)}, u32[]{:S(2)}, u32[]{:S(2)}) collective-permute-start(bf16[1,256,2048]{2,1,0:T(8,128)(2,1)} %refs_5_.1), channel_id=1, source_target_pairs={{0,1},{1,0},{2,3},{3,2},{4,5},{5,4},{6,7},{7,6},{8,9},{9,8},{10,11... | collective-permute-start | bytes 3145736 | tf_op jit(solution)/shard_map/ppermute | solution.py:159
  31.0 20.4 %collective-permute-start = (bf16[32,2176]{1,0:T(8,128)(2,1)}, bf16[32,2176]{1,0:T(8,128)(2,1)S(1)}, u32[]{:S(2)}, u32[]{:S(2)}) collective-permute-start(bf16[32,2176]{1,0:T(8,128)(2,1)} %get-tuple-element.28), channel_id=1, source_target_pairs={{0,2},{1,63},{2,4},{3,1},{4,6},{5,3},{6,8},{7,5},{8,10},{9,7},{10,... | collective-permute-start | bytes 417800 | tf_op jit(solution)/shard_map/ppermute | solution.py:155
  39.7 11.6 %collective-permute-start.9 = (bf16[32,2176]{1,0:T(8,128)(2,1)S(1)}, bf16[32,2176]{1,0:T(8,128)(2,1)S(1)}, u32[]{:S(2)}, u32[]{:S(2)}) collective-permute-start(bf16[32,2176]{1,0:T(8,128)(2,1)S(1)} %collective-permute-done.5.refs_6_), channel_id=1, source_target_pairs={{0,8},{1,57},{2,10},{3,59},{4,12},{5,61},{6,14},{7,63},{8,16},{9,1... | collective-permute-start | bytes 417800 | tf_op jit(solution)/shard_map/ppermute | solution.py:155
  51.4 8.5 %collective-permute-start.7 = (bf16[32,2176]{1,0:T(8,128)(2,1)S(1)}, bf16[32,2176]{1,0:T(8,128)(2,1)S(1)}, u32[]{:S(2)}, u32[]{:S(2)}) collective-permute-start(bf16[32,2176]{1,0:T(8,128)(2,1)S(1)} %collective-permute-done.5.refs_6_), channel_id=1, source_target_pairs={{0,4},{1,61},{2,6},{3,63},{4,8},{5,1},{6,10},{7,3},{8,12},{9,5},{1... | collective-permute-start | bytes 417800 | tf_op jit(solution)/shard_map/ppermute | solution.py:155
  51.4 8.9 %collective-permute-start.6 = (bf16[32,2176]{1,0:T(8,128)(2,1)S(1)}, bf16[32,2176]{1,0:T(8,128)(2,1)S(1)}, u32[]{:S(2)}, u32[]{:S(2)}) collective-permute-start(bf16[32,2176]{1,0:T(8,128)(2,1)S(1)} %collective-permute-done.5.refs_6_), channel_id=1, source_target_pairs={{0,2},{1,63},{2,4},{3,1},{4,6},{5,3},{6,8},{7,5},{8,10},{9,7},{10,... | collective-permute-start | bytes 417800 | tf_op jit(solution)/shard_map/ppermute | solution.py:155
  66.1 8.9 %collective-permute-start.12 = (bf16[32,2176]{1,0:T(8,128)(2,1)S(1)}, bf16[32,2176]{1,0:T(8,128)(2,1)S(1)}, u32[]{:S(2)}, u32[]{:S(2)}) collective-permute-start(bf16[32,2176]{1,0:T(8,128)(2,1)S(1)} %collective-permute-done.9.refs_10_), channel_id=1, source_target_pairs={{0,6},{1,59},{2,8},{3,61},{4,10},{5,63},{6,12},{7,1},{8,14},{9,3},... | collective-permute-start | bytes 417800 | tf_op jit(solution)/shard_map/ppermute | solution.py:155
  67.6 8.4 %collective-permute-start.10 = (bf16[32,2176]{1,0:T(8,128)(2,1)S(1)}, bf16[32,2176]{1,0:T(8,128)(2,1)S(1)}, u32[]{:S(2)}, u32[]{:S(2)}) collective-permute-start(bf16[32,2176]{1,0:T(8,128)(2,1)S(1)} %collective-permute-done.9.refs_10_), channel_id=1, source_target_pairs={{0,2},{1,63},{2,4},{3,1},{4,6},{5,3},{6,8},{7,5},{8,10},{9,7},{10,... | collective-permute-start | bytes 417800 | tf_op jit(solution)/shard_map/ppermute | solution.py:155
  103.9 9.0 %collective-permute-start.20 = (bf16[32,2048]{1,0:T(8,128)(2,1)S(1)}, bf16[32,2048]{1,0:T(8,128)(2,1)S(1)}, u32[]{:S(2)}, u32[]{:S(2)}) collective-permute-start(bf16[32,2048]{1,0:T(8,128)(2,1)S(1)} %get-tuple-element.37), channel_id=1, source_target_pairs={{0,62},{1,3},{2,0},{3,5},{4,2},{5,7},{6,4},{7,9},{8,6},{9,11},{10,... | collective-permute-start | bytes 393224 | tf_op jit(solution)/shard_map/ppermute | solution.py:155
  104.7 9.3 %collective-permute-start.22 = (bf16[32,2048]{1,0:T(8,128)(2,1)S(1)}, bf16[32,2048]{1,0:T(8,128)(2,1)S(1)}, u32[]{:S(2)}, u32[]{:S(2)}) collective-permute-start(bf16[32,2048]{1,0:T(8,128)(2,1)S(1)} %get-tuple-element.39), channel_id=1, source_target_pairs={{0,60},{1,5},{2,62},{3,7},{4,0},{5,9},{6,2},{7,11},{8,4},{9,13},{1... | collective-permute-start | bytes 393224 | tf_op jit(solution)/shard_map/ppermute | solution.py:155
  107.9 9.3 %collective-permute-start.23 = (bf16[32,2048]{1,0:T(8,128)(2,1)S(1)}, bf16[32,2048]{1,0:T(8,128)(2,1)S(1)}, u32[]{:S(2)}, u32[]{:S(2)}) collective-permute-start(bf16[32,2048]{1,0:T(8,128)(2,1)S(1)} %get-tuple-element.40), channel_id=1, source_target_pairs={{0,62},{1,3},{2,0},{3,5},{4,2},{5,7},{6,4},{7,9},{8,6},{9,11},{10,... | collective-permute-start | bytes 393224 | tf_op jit(solution)/shard_map/ppermute | solution.py:155
  108.7 25.4 %collective-permute-start.26 = (bf16[32,2048]{1,0:T(8,128)(2,1)S(1)}, bf16[32,2048]{1,0:T(8,128)(2,1)S(1)}, u32[]{:S(2)}, u32[]{:S(2)}) collective-permute-start(bf16[32,2048]{1,0:T(8,128)(2,1)S(1)} %get-tuple-element.42), channel_id=1, source_target_pairs={{0,62},{1,3},{2,0},{3,5},{4,2},{5,7},{6,4},{7,9},{8,6},{9,11},{10,... | collective-permute-start | bytes 393224 | tf_op jit(solution)/shard_map/ppermute | solution.py:155
  109.9 10.3 %collective-permute-start.27 = (bf16[32,2048]{1,0:T(8,128)(2,1)S(1)}, bf16[32,2048]{1,0:T(8,128)(2,1)S(1)}, u32[]{:S(2)}, u32[]{:S(2)}) collective-permute-start(bf16[32,2048]{1,0:T(8,128)(2,1)S(1)} %get-tuple-element.44), channel_id=1, source_target_pairs={{0,62},{1,3},{2,0},{3,5},{4,2},{5,7},{6,4},{7,9},{8,6},{9,11},{10,... | collective-permute-start | bytes 393224 | tf_op jit(solution)/shard_map/ppermute | solution.py:155
  112.9 23.5 %collective-permute-start.31 = (bf16[32,2048]{1,0:T(8,128)(2,1)S(1)}, bf16[32,2048]{1,0:T(8,128)(2,1)S(1)}, u32[]{:S(2)}, u32[]{:S(2)}) collective-permute-start(bf16[32,2048]{1,0:T(8,128)(2,1)S(1)} %get-tuple-element.46), channel_id=1, source_target_pairs={{0,62},{1,3},{2,0},{3,5},{4,2},{5,7},{6,4},{7,9},{8,6},{9,11},{10,... | collective-permute-start | bytes 393224 | tf_op jit(solution)/shard_map/ppermute | solution.py:155
  117.2 11.9 %collective-permute-start.21 = (bf16[32,2048]{1,0:T(8,128)(2,1)S(1)}, bf16[32,2048]{1,0:T(8,128)(2,1)S(1)}, u32[]{:S(2)}, u32[]{:S(2)}) collective-permute-start(bf16[32,2048]{1,0:T(8,128)(2,1)S(1)} %add_convert_fusion.9), channel_id=1, source_target_pairs={{0,56},{1,9},{2,58},{3,11},{4,60},{5,13},{6,62},{7,15},{8,0},{9,17... | collective-permute-start | bytes 393224 | tf_op jit(solution)/shard_map/ppermute | solution.py:155
  120.2 8.9 %collective-permute-start.24 = (bf16[32,2048]{1,0:T(8,128)(2,1)S(1)}, bf16[32,2048]{1,0:T(8,128)(2,1)S(1)}, u32[]{:S(2)}, u32[]{:S(2)}) collective-permute-start(bf16[32,2048]{1,0:T(8,128)(2,1)S(1)} %add_convert_fusion.8), channel_id=1, source_target_pairs={{0,62},{1,3},{2,0},{3,5},{4,2},{5,7},{6,4},{7,9},{8,6},{9,11},{10,... | collective-permute-start | bytes 393224 | tf_op jit(solution)/shard_map/ppermute | solution.py:155
  121.5 12.6 %collective-permute-start.28 = (bf16[32,2048]{1,0:T(8,128)(2,1)S(1)}, bf16[32,2048]{1,0:T(8,128)(2,1)S(1)}, u32[]{:S(2)}, u32[]{:S(2)}) collective-permute-start(bf16[32,2048]{1,0:T(8,128)(2,1)S(1)} %add_convert_fusion.6), channel_id=1, source_target_pairs={{0,60},{1,5},{2,62},{3,7},{4,0},{5,9},{6,2},{7,11},{8,4},{9,13},{1... | collective-permute-start | bytes 393224 | tf_op jit(solution)/shard_map/ppermute | solution.py:155
  129.2 13.0 %collective-permute-start.25 = (bf16[32,2048]{1,0:T(8,128)(2,1)S(1)}, bf16[32,2048]{1,0:T(8,128)(2,1)S(1)}, u32[]{:S(2)}, u32[]{:S(2)}) collective-permute-start(bf16[32,2048]{1,0:T(8,128)(2,1)S(1)} %add_convert_fusion.7), channel_id=1, source_target_pairs={{0,54},{1,11},{2,56},{3,13},{4,58},{5,15},{6,60},{7,17},{8,62},{9,... | collective-permute-start | bytes 393224 | tf_op jit(solution)/shard_map/ppermute | solution.py:155
  134.2 8.0 %collective-permute-start.29 = (bf16[32,2048]{1,0:T(8,128)(2,1)S(1)}, bf16[32,2048]{1,0:T(8,128)(2,1)S(1)}, u32[]{:S(2)}, u32[]{:S(2)}) collective-permute-start(bf16[32,2048]{1,0:T(8,128)(2,1)S(1)} %add_convert_fusion.5), channel_id=1, source_target_pairs={{0,62},{1,3},{2,0},{3,5},{4,2},{5,7},{6,4},{7,9},{8,6},{9,11},{10,... | collective-permute-start | bytes 393224 | tf_op jit(solution)/shard_map/ppermute | solution.py:155
  136.4 13.6 %collective-permute-start.34 = (bf16[32,2048]{1,0:T(8,128)(2,1)S(1)}, bf16[32,2048]{1,0:T(8,128)(2,1)S(1)}, u32[]{:S(2)}, u32[]{:S(2)}) collective-permute-start(bf16[32,2048]{1,0:T(8,128)(2,1)S(1)} %add_convert_fusion.2), channel_id=1, source_target_pairs={{0,62},{1,3},{2,0},{3,5},{4,2},{5,7},{6,4},{7,9},{8,6},{9,11},{10,... | collective-permute-start | bytes 393224 | tf_op jit(solution)/shard_map/ppermute | solution.py:155
  142.2 15.8 %collective-permute-start.30 = (bf16[32,2048]{1,0:T(8,128)(2,1)S(1)}, bf16[32,2048]{1,0:T(8,128)(2,1)S(1)}, u32[]{:S(2)}, u32[]{:S(2)}) collective-permute-start(bf16[32,2048]{1,0:T(8,128)(2,1)S(1)} %add_convert_fusion.4), channel_id=1, source_target_pairs={{0,54},{1,11},{2,56},{3,13},{4,58},{5,15},{6,60},{7,17},{8,62},{9,... | collective-permute-start | bytes 393224 | tf_op jit(solution)/shard_map/ppermute | solution.py:155
  (16 other events, 86.3 us)
where the time goes:
time: 161 us; the launch traced here: 160 us
  waiting for transfers between devices  80 us (50%)
  starting transfers between devices  69.7 us (43%)
  Pallas kernels  8.29 us (5%)
    ppermute x32, waiting for transfers between devices, turned(): return lax.ppermute(array, ('ep', 'tp'), pairs)  78.7 us
    ppermute x32, starting transfers between devices, turned(): return lax.ppermute(array, ('ep', 'tp'), pairs)  59.3 us
    ppermute x4, starting transfers between devices, swapped(): return lax.ppermute(array, 'tp', [(0, 1), (1, 0)])  10.4 us
    pallas_call x1, Pallas kernels, expert(): pl.pallas_call(functools.partial(second_kernel, n), out_shape=[jax.ShapeD...  3.4 us
  transfers between devices with their start and end apart: 36, of which 22 were waited for; matrix products, arithmetic and copies ran while one was open for 0% of the time, Pallas kernels for 0%

commit v1 on v0

v1 whole, which is shorter than its diff:
```python
import functools

import jax
import jax.numpy as jnp
from jax import lax
from jax.experimental import pallas as pl
from jax.experimental.pallas import tpu as pltpu
from jax.sharding import PartitionSpec as P


LANES = 128
GROUPS = 2
GATHER = (0, 1, 0, 3, 4, 0, 6, 6, 8, 6, 10, 11, 10, 13, 13, 15)
GATHER_ORDER = (6, 1, 3, 10, 8, 4, 7, 13, 11, 5, 2, 15, 14, 12, 9, 16)
COMBINE = (0, 1, 0, 1, 4, 4, 0, 7, 7, 9, 7, 11, 11, 11, 14, 14)
COMBINE_ORDER = (16, 15, 13, 10, 14, 12, 9, 6, 5, 11, 8, 3, 4, 2, 7, 1)
LAST = len(GATHER)


def own_group():
    return lax.axis_index("ep") // (lax.axis_size("ep") // GROUPS)


def turned_dot(a, b):
    return lax.dot_general(a, b, (((1,), (1,)), ((), ())), preferred_element_type=jnp.float32)


def prepare_kernel(tokens, gain, prob, logits, ids, unit, kept, back):
    rows, model = tokens.shape
    width = unit.shape[1]
    half = rows // GROUPS
    values = tokens[...].astype(jnp.float32)
    scale = lax.rsqrt(jnp.mean(values * values, axis=-1, keepdims=True) + 1e-06)
    normed = (values * scale * gain[...]).astype(jnp.bfloat16)
    expw = jnp.exp(logits[...])
    route_w = prob[...] * expw / jnp.sum(expw, axis=0, keepdims=True)
    picks, count = expw.shape
    experts = lax.axis_size("ep")
    expert = lax.broadcasted_iota(jnp.int32, (experts, count), 0)
    dense = jnp.zeros((experts, count), jnp.float32)
    for k in range(picks):
        dense += jnp.where(ids[k : k + 1, :] == expert, route_w[k : k + 1, :], 0.0)
    high = dense.astype(jnp.bfloat16).astype(jnp.float32)
    low = dense - high
    table = jnp.concatenate(
        [high, low, jnp.zeros((width - model - 2 * experts, count), jnp.float32)], axis=0
    ).astype(jnp.bfloat16)
    row = lax.broadcasted_iota(jnp.int32, (rows, count), 0)
    column = lax.broadcasted_iota(jnp.int32, (rows, count), 1)
    late = jnp.broadcast_to(ids[:1, :] >= experts // GROUPS, (rows, count))
    earlier = (row < column).astype(jnp.bfloat16)
    before = jnp.dot(
        late.astype(jnp.bfloat16), earlier, preferred_element_type=jnp.float32
    ).astype(jnp.int32)
    place = jnp.where(late, half + before, column - before)
    chosen = (place == row).astype(jnp.bfloat16)
    unit[:, :model] = jnp.dot(
        chosen, normed, preferred_element_type=jnp.float32
    ).astype(jnp.bfloat16)
    unit[:, model:] = turned_dot(chosen, table).astype(jnp.bfloat16)
    kept[...] = unit[pl.ds(pl.multiple_of(own_group() * half, half), half), :]
    back[...] = turned_dot((row == column).astype(jnp.bfloat16), chosen)


def block(x, gate_w, up_w, down_w):
    gate = jnp.dot(x, gate_w[0], preferred_element_type=jnp.float32)
    up = jnp.dot(x, up_w[0], preferred_element_type=jnp.float32)
    act = (gate / (1.0 + jnp.exp(-gate)) * up).astype(jnp.bfloat16)
    return jnp.dot(act, down_w[0], preferred_element_type=jnp.float32).astype(jnp.bfloat16)


def first_kernel(n, *refs):
    units, other, (rows_all, weight_all, part_all) = refs[:n], refs[n : n + 3], refs[n + 3 :]
    half, _ = units[0].shape
    model = rows_all.shape[1]
    me, core = lax.axis_index("ep"), lax.axis_index("tp")
    experts = lax.axis_size("ep")
    group = own_group()
    for k, unit in enumerate(units):
        if unit.shape[0] == half:
            some = slice(None)
        else:
            some = pl.ds(pl.multiple_of(group * half, half), half)
        at = slice(k * half, (k + 1) * half)
        rows_all[at, :] = unit[some, :model]
        table = unit[some, model:].astype(jnp.float32)
        lane = lax.broadcasted_iota(jnp.int32, table.shape, 1)
        mine = (lane == me) | (lane == me + experts)
        if k in (0, n - 1):
            mine = mine & (core == (0 if k == 0 else 1))
        taken = jnp.where(mine, table, 0.0)
        weight_all[at, :] = jnp.broadcast_to(jnp.sum(taken, axis=1, keepdims=True), table.shape)
    part_all[...] = block(rows_all[...], *other)


def second_kernel(n, *refs):
    (rows_all, weight_all, part_all, *own), outs = refs[:6], refs[6:]
    half = outs[0].shape[0]
    part = block(rows_all[...], *own).astype(jnp.float32)
    total = (part_all[...].astype(jnp.float32) + part).astype(jnp.bfloat16)
    weighted = (total.astype(jnp.float32) * weight_all[:, :1]).astype(jnp.bfloat16)
    for k in range(n):
        outs[k][...] = weighted[k * half : (k + 1) * half]


VMEM = pl.BlockSpec(memory_space=pltpu.VMEM)


def prepare(tokens, norm_gain, group_prob, route_logits, expert_ids):
    rows, model = tokens.shape
    width = model + LANES
    return pl.pallas_call(
        prepare_kernel,
        out_shape=[
            jax.ShapeDtypeStruct((rows, width), jnp.bfloat16),
            jax.ShapeDtypeStruct((rows // GROUPS, width), jnp.bfloat16),
            jax.ShapeDtypeStruct((rows, rows), jnp.float32),
        ],
        in_specs=[VMEM] * 5,
        out_specs=[VMEM] * 3,
        name="prepare",
    )(tokens, norm_gain[None, :], group_prob[None, :], route_logits.T, expert_ids.T)


def expert(units, own, other):
    n = len(units)
    half, width = units[0].shape
    model = width - LANES
    total = n * half
    params = pltpu.CompilerParams(vmem_limit_bytes=20 * 1024 * 1024)
    whole = jax.ShapeDtypeStruct((total, model), jnp.bfloat16)
    held = pl.pallas_call(
        functools.partial(first_kernel, n),
        out_shape=[whole, jax.ShapeDtypeStruct((total, LANES), jnp.float32), whole],
        in_specs=[VMEM] * (n + 3),
        out_specs=[VMEM] * 3,
        compiler_params=params,
        name="first",
    )(*units, *other)
    return pl.pallas_call(
        functools.partial(second_kernel, n),
        out_shape=[jax.ShapeDtypeStruct((half, model), jnp.bfloat16)] * n,
        in_specs=[VMEM] * 6,
        out_specs=[VMEM] * n,
        compiler_params=params,
        name="second",
    )(*held, *own)


def finish(here, there, back):
    total = (here.astype(jnp.float32) + there.astype(jnp.float32)).astype(jnp.bfloat16)
    return jnp.dot(
        back.astype(jnp.bfloat16), total, preferred_element_type=jnp.float32
    ).astype(jnp.bfloat16)


def turned(array, shift):
    n, cores = lax.axis_size("ep"), lax.axis_size("tp")
    pairs = []
    for i in range(n):
        for core in range(cores):
            to = (i + (shift if core == 0 else -shift)) % n
            pairs.append((i * cores + core, to * cores + core))
    return lax.ppermute(array, ("ep", "tp"), pairs)


def swapped(array):
    return lax.ppermute(array, "tp", [(0, 1), (1, 0)])


def node_kernel(distances, *refs):
    *parts, out, total = refs
    half = out.shape[0] // GROUPS
    n = lax.axis_size("ep")
    me, side = lax.axis_index("ep"), 1 - 2 * lax.axis_index("tp")
    total[...] = jnp.zeros_like(total)
    for part, distance in zip(parts, distances):
        values = part[...].astype(jnp.float32)
        if distance is None:
            total[...] += values
        else:
            group = lax.rem(me + side * distance + n, n) // (n // GROUPS)
            total[pl.ds(pl.multiple_of(group * half, half), half), :] += values
    out[...] = total[...].astype(out.dtype)


def added(parts):
    arrays, distances = zip(*parts)
    half, model = arrays[0].shape
    shape = (GROUPS * half, model)
    return pl.pallas_call(
        functools.partial(node_kernel, distances),
        out_shape=jax.ShapeDtypeStruct(shape, jnp.bfloat16),
        in_specs=[VMEM] * len(arrays),
        out_specs=VMEM,
        scratch_shapes=[pltpu.VMEM(shape, jnp.float32)],
        compiler_params=pltpu.CompilerParams(vmem_limit_bytes=8 * 1024 * 1024),
        name="node",
    )(*arrays)


def gather(unit):
    held = {0: unit}
    for at in GATHER_ORDER:
        by = GATHER[at - 1]
        held[at] = turned(held[by], at - by)
    return [held[at] for at in range(LAST + 1)]


def combine(outs):
    parts = {at: [(out, 0)] for at, out in enumerate(outs)}
    for at in COMBINE_ORDER:
        by = COMBINE[at - 1]
        sent = added(parts[at]) if at in COMBINE else outs[at]
        came = turned(sent, by - at)
        parts[by].append((came, None if at in COMBINE else at - by))
    return added(parts[0])


def shards(tokens, norm_gain, group_prob, route_logits, expert_ids, w_gate, w_up, w_down):
    own, other = (w_gate, w_up, w_down), []
    for w in own:
        other.append(swapped(w))
    unit, kept, back = prepare(tokens, norm_gain, group_prob, route_logits, expert_ids)
    units = gather(unit)
    mixed = combine(expert([kept, *units[1:]], own, other))
    return finish(mixed, swapped(mixed), back)


def solution(mesh):
    in_specs = (
        P(("grp", "ep"), None),
        P(),
        P(("grp", "ep")),
        P(("grp", "ep"), None),
        P(("grp", "ep"), None),
        P("ep", None, "tp"),
        P("ep", None, "tp"),
        P("ep", "tp", None),
    )
    out_specs = P(("grp", "ep"), None)
    return jax.shard_map(
        shards, mesh=mesh, in_specs=in_specs, out_specs=out_specs, check_vma=False
    )
```

time: 161 us -> 162 us (level)
  waiting for transfers between devices: 80 us -> 86.1 us
  Pallas kernels: 8.29 us -> 4.99 us
    ppermute x32, waiting for transfers between devices: 78.7 us -> 84.8 us  [turned(): return lax.ppermute(array, ('ep', 'tp'), pairs)]
    pallas_call x1, Pallas kernels: 3.4 us -> 1.38 us  [expert(): pl.pallas_call(functools.partial(second_kernel, n), out_shape=[jax.ShapeD...]
    pallas_call x1, Pallas kernels: 3.08 us -> 1.14 us  [expert(): pl.pallas_call(functools.partial(first_kernel, n), out_shape=[whole, jax....]
    ppermute x32, starting transfers between devices: 59.3 us -> 57.7 us  [turned(): return lax.ppermute(array, ('ep', 'tp'), pairs)]
  transfers between devices with their start and end apart: 36 -> 36, of which waited for: 22 -> 21; matrix products, arithmetic and copies ran while one was open for 0% -> 0% of each run, Pallas kernels for 0% -> 0%
where the time goes in v1:
time: 162 us
  waiting for transfers between devices  86.1 us (53%)
  starting transfers between devices  68.1 us (42%)
  Pallas kernels  4.99 us (3%)
    ppermute x32, waiting for transfers between devices, turned(): return lax.ppermute(array, ('ep', 'tp'), pairs)  84.8 us
    ppermute x32, starting transfers between devices, turned(): return lax.ppermute(array, ('ep', 'tp'), pairs)  57.7 us
    ppermute x4, starting transfers between devices, swapped(): return lax.ppermute(array, 'tp', [(0, 1), (1, 0)])  10.4 us
  transfers between devices with their start and end apart: 36, of which 21 were waited for; matrix products, arithmetic and copies ran while one was open for 0% of the time, Pallas kernels for 0%

profile of v1, /device:TPU:38, one launch (start us, length us, event | category | flops | bytes accessed | tf_op | source)
XLA Modules:
  0.0 161.8 jit_solution(6921382783563253737)
XLA Ops:
  1.9 11.1 %collective-permute-start.5 = (bf16[32,2176]{1,0:T(8,128)(2,1)}, bf16[32,2176]{1,0:T(8,128)(2,1)S(1)}, u32[]{:S(2)}, u32[]{:S(2)}) collective-permute-start(bf16[32,2176]{1,0:T(8,128)(2,1)} %get-tuple-element.30), channel_id=1, source_target_pairs={{0,12},{1,53},{2,14},{3,55},{4,16},{5,57},{6,18},{7,59},{8,20},{9,... | collective-permute-start | bytes 417800 | tf_op jit(solution)/shard_map/ppermute | solution.py:164
  13.0 6.4 %collective-permute-start.2 = (bf16[32,2176]{1,0:T(8,128)(2,1)}, bf16[32,2176]{1,0:T(8,128)(2,1)S(1)}, u32[]{:S(2)}, u32[]{:S(2)}) collective-permute-start(bf16[32,2176]{1,0:T(8,128)(2,1)} %get-tuple-element.30), channel_id=1, source_target_pairs={{0,6},{1,59},{2,8},{3,61},{4,10},{5,63},{6,12},{7,1},{8,14},{9,3},... | collective-permute-start | bytes 417800 | tf_op jit(solution)/shard_map/ppermute | solution.py:164
  19.5 9.7 %collective-permute-start.16 = (bf16[1,2048,256]{2,1,0:T(8,128)(2,1)}, bf16[1,2048,256]{2,1,0:T(8,128)(2,1)S(1)}, u32[]{:S(2)}, u32[]{:S(2)}) collective-permute-start(bf16[1,2048,256]{2,1,0:T(8,128)(2,1)} %refs_3_.1), channel_id=1, source_target_pairs={{0,1},{1,0},{2,3},{3,2},{4,5},{5,4},{6,7},{7,6},{8,9},{9,8},{10,11... | collective-permute-start | bytes 3145736 | tf_op jit(solution)/shard_map/ppermute | solution.py:168
  31.1 4.1 %collective-permute-start = (bf16[32,2176]{1,0:T(8,128)(2,1)}, bf16[32,2176]{1,0:T(8,128)(2,1)S(1)}, u32[]{:S(2)}, u32[]{:S(2)}) collective-permute-start(bf16[32,2176]{1,0:T(8,128)(2,1)} %get-tuple-element.30), channel_id=1, source_target_pairs={{0,2},{1,63},{2,4},{3,1},{4,6},{5,3},{6,8},{7,5},{8,10},{9,7},{10,... | collective-permute-start | bytes 417800 | tf_op jit(solution)/shard_map/ppermute | solution.py:164
  35.2 4.6 %collective-permute-done.2.refs_3_ = bf16[32,2176]{1,0:T(8,128)(2,1)S(1)} collective-permute-done((bf16[32,2176]{1,0:T(8,128)(2,1)}, bf16[32,2176]{1,0:T(8,128)(2,1)S(1)}, u32[]{:S(2)}, u32[]{:S(2)}) %collective-permute-start.2) | collective-permute-done | bytes 139296 | tf_op jit(solution)/shard_map/ppermute | solution.py:164
  39.9 4.9 %collective-permute-start.9 = (bf16[32,2176]{1,0:T(8,128)(2,1)S(1)}, bf16[32,2176]{1,0:T(8,128)(2,1)S(1)}, u32[]{:S(2)}, u32[]{:S(2)}) collective-permute-start(bf16[32,2176]{1,0:T(8,128)(2,1)S(1)} %collective-permute-done.5.refs_6_), channel_id=1, source_target_pairs={{0,8},{1,57},{2,10},{3,59},{4,12},{5,61},{6,14},{7,63},{8,16},{9,1... | collective-permute-start | bytes 417800 | tf_op jit(solution)/shard_map/ppermute | solution.py:164
  44.8 6.7 %collective-permute-done.refs_1_ = bf16[32,2176]{1,0:T(8,128)(2,1)S(1)} collective-permute-done((bf16[32,2176]{1,0:T(8,128)(2,1)}, bf16[32,2176]{1,0:T(8,128)(2,1)S(1)}, u32[]{:S(2)}, u32[]{:S(2)}) %collective-permute-start) | collective-permute-done | bytes 139296 | tf_op jit(solution)/shard_map/ppermute | solution.py:164
  51.5 8.5 %collective-permute-done.7.refs_8_ = bf16[32,2176]{1,0:T(8,128)(2,1)S(1)} collective-permute-done((bf16[32,2176]{1,0:T(8,128)(2,1)S(1)}, bf16[32,2176]{1,0:T(8,128)(2,1)S(1)}, u32[]{:S(2)}, u32[]{:S(2)}) %collective-permute-start.7) | collective-permute-done | bytes 139296 | tf_op jit(solution)/shard_map/ppermute | solution.py:164
  60.4 5.8 %collective-permute-done.3.refs_4_ = bf16[32,2176]{1,0:T(8,128)(2,1)S(1)} collective-permute-done((bf16[32,2176]{1,0:T(8,128)(2,1)S(1)}, bf16[32,2176]{1,0:T(8,128)(2,1)S(1)}, u32[]{:S(2)}, u32[]{:S(2)}) %collective-permute-start.3) | collective-permute-done | bytes 139296 | tf_op jit(solution)/shard_map/ppermute | solution.py:164
  67.7 7.4 %collective-permute-done.12.refs_13_ = bf16[32,2176]{1,0:T(8,128)(2,1)S(1)} collective-permute-done((bf16[32,2176]{1,0:T(8,128)(2,1)S(1)}, bf16[32,2176]{1,0:T(8,128)(2,1)S(1)}, u32[]{:S(2)}, u32[]{:S(2)}) %collective-permute-start.12) | collective-permute-done | bytes 139296 | tf_op jit(solution)/shard_map/ppermute | solution.py:164
  76.1 5.2 %collective-permute-done.8.refs_9_ = bf16[32,2176]{1,0:T(8,128)(2,1)S(1)} collective-permute-done((bf16[32,2176]{1,0:T(8,128)(2,1)S(1)}, bf16[32,2176]{1,0:T(8,128)(2,1)S(1)}, u32[]{:S(2)}, u32[]{:S(2)}) %collective-permute-start.8) | collective-permute-done | bytes 139296 | tf_op jit(solution)/shard_map/ppermute | solution.py:164
  82.9 5.8 %collective-permute-done.14.refs_15_ = bf16[32,2176]{1,0:T(8,128)(2,1)S(1)} collective-permute-done((bf16[32,2176]{1,0:T(8,128)(2,1)S(1)}, bf16[32,2176]{1,0:T(8,128)(2,1)S(1)}, u32[]{:S(2)}, u32[]{:S(2)}) %collective-permute-start.14) | collective-permute-done | bytes 139296 | tf_op jit(solution)/shard_map/ppermute | solution.py:164
  90.0 5.5 %collective-permute-done.11.refs_12_ = bf16[32,2176]{1,0:T(8,128)(2,1)S(1)} collective-permute-done((bf16[32,2176]{1,0:T(8,128)(2,1)S(1)}, bf16[32,2176]{1,0:T(8,128)(2,1)S(1)}, u32[]{:S(2)}, u32[]{:S(2)}) %collective-permute-start.11) | collective-permute-done | bytes 139296 | tf_op jit(solution)/shard_map/ppermute | solution.py:164
  95.5 4.3 %collective-permute-done.15.refs_16_ = bf16[32,2176]{1,0:T(8,128)(2,1)S(1)} collective-permute-done((bf16[32,2176]{1,0:T(8,128)(2,1)S(1)}, bf16[32,2176]{1,0:T(8,128)(2,1)S(1)}, u32[]{:S(2)}, u32[]{:S(2)}) %collective-permute-start.15) | collective-permute-done | bytes 139296 | tf_op jit(solution)/shard_map/ppermute | solution.py:164
  104.7 4.6 %collective-permute-done.23.refs_1_ = bf16[16,2048]{1,0:T(8,128)(2,1)S(1)} collective-permute-done((bf16[16,2048]{1,0:T(8,128)(2,1)S(1)}, bf16[16,2048]{1,0:T(8,128)(2,1)S(1)}, u32[]{:S(2)}, u32[]{:S(2)}) %collective-permute-start.23) | collective-permute-done | bytes 65568 | tf_op jit(solution)/shard_map/ppermute | solution.py:164
  112.0 3.9 %collective-permute-start.22 = (bf16[16,2048]{1,0:T(8,128)(2,1)S(1)}, bf16[16,2048]{1,0:T(8,128)(2,1)S(1)}, u32[]{:S(2)}, u32[]{:S(2)}) collective-permute-start(bf16[16,2048]{1,0:T(8,128)(2,1)S(1)} %get-tuple-element.40), channel_id=1, source_target_pairs={{0,60},{1,5},{2,62},{3,7},{4,0},{5,9},{6,2},{7,11},{8,4},{9,13},{1... | collective-permute-start | bytes 196616 | tf_op jit(solution)/shard_map/ppermute | solution.py:164
  118.2 2.3 %collective-permute-start.32 = (bf16[32,2048]{1,0:T(8,128)(2,1)S(1)}, bf16[32,2048]{1,0:T(8,128)(2,1)S(1)}, u32[]{:S(2)}, u32[]{:S(2)}) collective-permute-start(bf16[32,2048]{1,0:T(8,128)(2,1)S(1)} %node.11), channel_id=1, source_target_pairs={{0,58},{1,7},{2,60},{3,9},{4,62},{5,11},{6,0},{7,13},{8,2},{9,15},... | collective-permute-start | bytes 393224 | tf_op jit(solution)/shard_map/ppermute | solution.py:164
  120.6 3.7 %collective-permute-start.21 = (bf16[32,2048]{1,0:T(8,128)(2,1)S(1)}, bf16[32,2048]{1,0:T(8,128)(2,1)S(1)}, u32[]{:S(2)}, u32[]{:S(2)}) collective-permute-start(bf16[32,2048]{1,0:T(8,128)(2,1)S(1)} %node.7), channel_id=1, source_target_pairs={{0,60},{1,5},{2,62},{3,7},{4,0},{5,9},{6,2},{7,11},{8,4},{9,13},{1... | collective-permute-start | bytes 393224 | tf_op jit(solution)/shard_map/ppermute | solution.py:164
  124.4 5.4 %collective-permute-start.27 = (bf16[32,2048]{1,0:T(8,128)(2,1)S(1)}, bf16[32,2048]{1,0:T(8,128)(2,1)S(1)}, u32[]{:S(2)}, u32[]{:S(2)}) collective-permute-start(bf16[32,2048]{1,0:T(8,128)(2,1)S(1)} %node.9), channel_id=1, source_target_pairs={{0,56},{1,9},{2,58},{3,11},{4,60},{5,13},{6,62},{7,15},{8,0},{9,17... | collective-permute-start | bytes 393224 | tf_op jit(solution)/shard_map/ppermute | solution.py:164
  130.4 5.4 %collective-permute-done.33.refs_2_ = bf16[16,2048]{1,0:T(8,128)(2,1)S(1)} collective-permute-done((bf16[16,2048]{1,0:T(8,128)(2,1)S(1)}, bf16[16,2048]{1,0:T(8,128)(2,1)S(1)}, u32[]{:S(2)}, u32[]{:S(2)}) %collective-permute-start.33) | collective-permute-done | bytes 65568 | tf_op jit(solution)/shard_map/ppermute | solution.py:164
  135.9 3.8 %collective-permute-start.34 = (bf16[32,2048]{1,0:T(8,128)(2,1)S(1)}, bf16[32,2048]{1,0:T(8,128)(2,1)S(1)}, u32[]{:S(2)}, u32[]{:S(2)}) collective-permute-start(bf16[32,2048]{1,0:T(8,128)(2,1)S(1)} %node.12), channel_id=1, source_target_pairs={{0,62},{1,3},{2,0},{3,5},{4,2},{5,7},{6,4},{7,9},{8,6},{9,11},{10,... | collective-permute-start | bytes 393224 | tf_op jit(solution)/shard_map/ppermute | solution.py:164
  139.8 3.6 %collective-permute-start.29 = (bf16[32,2048]{1,0:T(8,128)(2,1)S(1)}, bf16[32,2048]{1,0:T(8,128)(2,1)S(1)}, u32[]{:S(2)}, u32[]{:S(2)}) collective-permute-start(bf16[32,2048]{1,0:T(8,128)(2,1)S(1)} %node.10), channel_id=1, source_target_pairs={{0,50},{1,15},{2,52},{3,17},{4,54},{5,19},{6,56},{7,21},{8,58},{9,... | collective-permute-start | bytes 393224 | tf_op jit(solution)/shard_map/ppermute | solution.py:164
  143.4 3.5 %collective-permute-start.19 = (bf16[16,2048]{1,0:T(8,128)(2,1)S(1)}, bf16[16,2048]{1,0:T(8,128)(2,1)S(1)}, u32[]{:S(2)}, u32[]{:S(2)}) collective-permute-start(bf16[16,2048]{1,0:T(8,128)(2,1)S(1)} %get-tuple-element.35), channel_id=1, source_target_pairs={{0,58},{1,7},{2,60},{3,9},{4,62},{5,11},{6,0},{7,13},{8,2},{9,15},... | collective-permute-start | bytes 196616 | tf_op jit(solution)/shard_map/ppermute | solution.py:164
  146.9 10.5 %collective-permute-done.19.refs_1_ = bf16[16,2048]{1,0:T(8,128)(2,1)S(1)} collective-permute-done((bf16[16,2048]{1,0:T(8,128)(2,1)S(1)}, bf16[16,2048]{1,0:T(8,128)(2,1)S(1)}, u32[]{:S(2)}, u32[]{:S(2)}) %collective-permute-start.19) | collective-permute-done | bytes 65568 | tf_op jit(solution)/shard_map/ppermute | solution.py:164
  (69 shorter events, 24.8 us)
Async XLA Ops:
  1.9 29.2 %collective-permute-start.5 = (bf16[32,2176]{1,0:T(8,128)(2,1)}, bf16[32,2176]{1,0:T(8,128)(2,1)S(1)}, u32[]{:S(2)}, u32[]{:S(2)}) collective-permute-start(bf16[32,2176]{1,0:T(8,128)(2,1)} %get-tuple-element.30), channel_id=1, source_target_pairs={{0,12},{1,53},{2,14},{3,55},{4,16},{5,57},{6,18},{7,59},{8,20},{9,... | collective-permute-start | bytes 417800 | tf_op jit(solution)/shard_map/ppermute | solution.py:164
  13.0 26.8 %collective-permute-start.2 = (bf16[32,2176]{1,0:T(8,128)(2,1)}, bf16[32,2176]{1,0:T(8,128)(2,1)S(1)}, u32[]{:S(2)}, u32[]{:S(2)}) collective-permute-start(bf16[32,2176]{1,0:T(8,128)(2,1)} %get-tuple-element.30), channel_id=1, source_target_pairs={{0,6},{1,59},{2,8},{3,61},{4,10},{5,63},{6,12},{7,1},{8,14},{9,3},... | collective-permute-start | bytes 417800 | tf_op jit(solution)/shard_map/ppermute | solution.py:164
  19.5 80.3 %collective-permute-start.16 = (bf16[1,2048,256]{2,1,0:T(8,128)(2,1)}, bf16[1,2048,256]{2,1,0:T(8,128)(2,1)S(1)}, u32[]{:S(2)}, u32[]{:S(2)}) collective-permute-start(bf16[1,2048,256]{2,1,0:T(8,128)(2,1)} %refs_3_.1), channel_id=1, source_target_pairs={{0,1},{1,0},{2,3},{3,2},{4,5},{5,4},{6,7},{7,6},{8,9},{9,8},{10,11... | collective-permute-start | bytes 3145736 | tf_op jit(solution)/shard_map/ppermute | solution.py:168
  29.2 70.6 %collective-permute-start.17 = (bf16[1,2048,256]{2,1,0:T(8,128)(2,1)}, bf16[1,2048,256]{2,1,0:T(8,128)(2,1)S(1)}, u32[]{:S(2)}, u32[]{:S(2)}) collective-permute-start(bf16[1,2048,256]{2,1,0:T(8,128)(2,1)} %refs_4_.1), channel_id=1, source_target_pairs={{0,1},{1,0},{2,3},{3,2},{4,5},{5,4},{6,7},{7,6},{8,9},{9,8},{10,11... | collective-permute-start | bytes 3145736 | tf_op jit(solution)/shard_map/ppermute | solution.py:168
  29.2 70.6 %collective-permute-start.18 = (bf16[1,256,2048]{2,1,0:T(8,128)(2,1)}, bf16[1,256,2048]{2,1,0:T(8,128)(2,1)S(1)}, u32[]{:S(2)}, u32[]{:S(2)}) collective-permute-start(bf16[1,256,2048]{2,1,0:T(8,128)(2,1)} %refs_5_.1), channel_id=1, source_target_pairs={{0,1},{1,0},{2,3},{3,2},{4,5},{5,4},{6,7},{7,6},{8,9},{9,8},{10,11... | collective-permute-start | bytes 3145736 | tf_op jit(solution)/shard_map/ppermute | solution.py:168
  31.1 20.4 %collective-permute-start = (bf16[32,2176]{1,0:T(8,128)(2,1)}, bf16[32,2176]{1,0:T(8,128)(2,1)S(1)}, u32[]{:S(2)}, u32[]{:S(2)}) collective-permute-start(bf16[32,2176]{1,0:T(8,128)(2,1)} %get-tuple-element.30), channel_id=1, source_target_pairs={{0,2},{1,63},{2,4},{3,1},{4,6},{5,3},{6,8},{7,5},{8,10},{9,7},{10,... | collective-permute-start | bytes 417800 | tf_op jit(solution)/shard_map/ppermute | solution.py:164
  39.9 11.6 %collective-permute-start.9 = (bf16[32,2176]{1,0:T(8,128)(2,1)S(1)}, bf16[32,2176]{1,0:T(8,128)(2,1)S(1)}, u32[]{:S(2)}, u32[]{:S(2)}) collective-permute-start(bf16[32,2176]{1,0:T(8,128)(2,1)S(1)} %collective-permute-done.5.refs_6_), channel_id=1, source_target_pairs={{0,8},{1,57},{2,10},{3,59},{4,12},{5,61},{6,14},{7,63},{8,16},{9,1... | collective-permute-start | bytes 417800 | tf_op jit(solution)/shard_map/ppermute | solution.py:164
  51.5 8.5 %collective-permute-start.7 = (bf16[32,2176]{1,0:T(8,128)(2,1)S(1)}, bf16[32,2176]{1,0:T(8,128)(2,1)S(1)}, u32[]{:S(2)}, u32[]{:S(2)}) collective-permute-start(bf16[32,2176]{1,0:T(8,128)(2,1)S(1)} %collective-permute-done.5.refs_6_), channel_id=1, source_target_pairs={{0,4},{1,61},{2,6},{3,63},{4,8},{5,1},{6,10},{7,3},{8,12},{9,5},{1... | collective-permute-start | bytes 417800 | tf_op jit(solution)/shard_map/ppermute | solution.py:164
  51.5 8.9 %collective-permute-start.6 = (bf16[32,2176]{1,0:T(8,128)(2,1)S(1)}, bf16[32,2176]{1,0:T(8,128)(2,1)S(1)}, u32[]{:S(2)}, u32[]{:S(2)}) collective-permute-start(bf16[32,2176]{1,0:T(8,128)(2,1)S(1)} %collective-permute-done.5.refs_6_), channel_id=1, source_target_pairs={{0,2},{1,63},{2,4},{3,1},{4,6},{5,3},{6,8},{7,5},{8,10},{9,7},{10,... | collective-permute-start | bytes 417800 | tf_op jit(solution)/shard_map/ppermute | solution.py:164
  66.2 8.8 %collective-permute-start.12 = (bf16[32,2176]{1,0:T(8,128)(2,1)S(1)}, bf16[32,2176]{1,0:T(8,128)(2,1)S(1)}, u32[]{:S(2)}, u32[]{:S(2)}) collective-permute-start(bf16[32,2176]{1,0:T(8,128)(2,1)S(1)} %collective-permute-done.9.refs_10_), channel_id=1, source_target_pairs={{0,6},{1,59},{2,8},{3,61},{4,10},{5,63},{6,12},{7,1},{8,14},{9,3},... | collective-permute-start | bytes 417800 | tf_op jit(solution)/shard_map/ppermute | solution.py:164
  67.7 8.4 %collective-permute-start.10 = (bf16[32,2176]{1,0:T(8,128)(2,1)S(1)}, bf16[32,2176]{1,0:T(8,128)(2,1)S(1)}, u32[]{:S(2)}, u32[]{:S(2)}) collective-permute-start(bf16[32,2176]{1,0:T(8,128)(2,1)S(1)} %collective-permute-done.9.refs_10_), channel_id=1, source_target_pairs={{0,2},{1,63},{2,4},{3,1},{4,6},{5,3},{6,8},{7,5},{8,10},{9,7},{10,... | collective-permute-start | bytes 417800 | tf_op jit(solution)/shard_map/ppermute | solution.py:164
  90.0 9.8 %collective-permute-start.15 = (bf16[32,2176]{1,0:T(8,128)(2,1)S(1)}, bf16[32,2176]{1,0:T(8,128)(2,1)S(1)}, u32[]{:S(2)}, u32[]{:S(2)}) collective-permute-start(bf16[32,2176]{1,0:T(8,128)(2,1)S(1)} %collective-permute-done.14.refs_15_), channel_id=1, source_target_pairs={{0,2},{1,63},{2,4},{3,1},{4,6},{5,3},{6,8},{7,5},{8,10},{9,7},{10,... | collective-permute-start | bytes 417800 | tf_op jit(solution)/shard_map/ppermute | solution.py:164
  104.2 11.8 %collective-permute-start.30 = (bf16[16,2048]{1,0:T(8,128)(2,1)S(1)}, bf16[16,2048]{1,0:T(8,128)(2,1)S(1)}, u32[]{:S(2)}, u32[]{:S(2)}) collective-permute-start(bf16[16,2048]{1,0:T(8,128)(2,1)S(1)} %get-tuple-element.48), channel_id=1, source_target_pairs={{0,60},{1,5},{2,62},{3,7},{4,0},{5,9},{6,2},{7,11},{8,4},{9,13},{1... | collective-permute-start | bytes 196616 | tf_op jit(solution)/shard_map/ppermute | solution.py:164
  109.4 14.9 %collective-permute-start.25 = (bf16[32,2048]{1,0:T(8,128)(2,1)S(1)}, bf16[32,2048]{1,0:T(8,128)(2,1)S(1)}, u32[]{:S(2)}, u32[]{:S(2)}) collective-permute-start(bf16[32,2048]{1,0:T(8,128)(2,1)S(1)} %node.8), channel_id=1, source_target_pairs={{0,58},{1,7},{2,60},{3,9},{4,62},{5,11},{6,0},{7,13},{8,2},{9,15},... | collective-permute-start | bytes 393224 | tf_op jit(solution)/shard_map/ppermute | solution.py:164
  109.5 8.6 %collective-permute-start.31 = (bf16[16,2048]{1,0:T(8,128)(2,1)S(1)}, bf16[16,2048]{1,0:T(8,128)(2,1)S(1)}, u32[]{:S(2)}, u32[]{:S(2)}) collective-permute-start(bf16[16,2048]{1,0:T(8,128)(2,1)S(1)} %get-tuple-element.49), channel_id=1, source_target_pairs={{0,62},{1,3},{2,0},{3,5},{4,2},{5,7},{6,4},{7,9},{8,6},{9,11},{10,... | collective-permute-start | bytes 196616 | tf_op jit(solution)/shard_map/ppermute | solution.py:164
  111.3 9.3 %collective-permute-start.20 = (bf16[16,2048]{1,0:T(8,128)(2,1)S(1)}, bf16[16,2048]{1,0:T(8,128)(2,1)S(1)}, u32[]{:S(2)}, u32[]{:S(2)}) collective-permute-start(bf16[16,2048]{1,0:T(8,128)(2,1)S(1)} %get-tuple-element.38), channel_id=1, source_target_pairs={{0,62},{1,3},{2,0},{3,5},{4,2},{5,7},{6,4},{7,9},{8,6},{9,11},{10,... | collective-permute-start | bytes 196616 | tf_op jit(solution)/shard_map/ppermute | solution.py:164
  112.0 12.3 %collective-permute-start.22 = (bf16[16,2048]{1,0:T(8,128)(2,1)S(1)}, bf16[16,2048]{1,0:T(8,128)(2,1)S(1)}, u32[]{:S(2)}, u32[]{:S(2)}) collective-permute-start(bf16[16,2048]{1,0:T(8,128)(2,1)S(1)} %get-tuple-element.40), channel_id=1, source_target_pairs={{0,60},{1,5},{2,62},{3,7},{4,0},{5,9},{6,2},{7,11},{8,4},{9,13},{1... | collective-permute-start | bytes 196616 | tf_op jit(solution)/shard_map/ppermute | solution.py:164
  118.2 17.6 %collective-permute-start.32 = (bf16[32,2048]{1,0:T(8,128)(2,1)S(1)}, bf16[32,2048]{1,0:T(8,128)(2,1)S(1)}, u32[]{:S(2)}, u32[]{:S(2)}) collective-permute-start(bf16[32,2048]{1,0:T(8,128)(2,1)S(1)} %node.11), channel_id=1, source_target_pairs={{0,58},{1,7},{2,60},{3,9},{4,62},{5,11},{6,0},{7,13},{8,2},{9,15},... | collective-permute-start | bytes 393224 | tf_op jit(solution)/shard_map/ppermute | solution.py:164
  120.6 19.1 %collective-permute-start.21 = (bf16[32,2048]{1,0:T(8,128)(2,1)S(1)}, bf16[32,2048]{1,0:T(8,128)(2,1)S(1)}, u32[]{:S(2)}, u32[]{:S(2)}) collective-permute-start(bf16[32,2048]{1,0:T(8,128)(2,1)S(1)} %node.7), channel_id=1, source_target_pairs={{0,60},{1,5},{2,62},{3,7},{4,0},{5,9},{6,2},{7,11},{8,4},{9,13},{1... | collective-permute-start | bytes 393224 | tf_op jit(solution)/shard_map/ppermute | solution.py:164
  124.4 15.3 %collective-permute-start.27 = (bf16[32,2048]{1,0:T(8,128)(2,1)S(1)}, bf16[32,2048]{1,0:T(8,128)(2,1)S(1)}, u32[]{:S(2)}, u32[]{:S(2)}) collective-permute-start(bf16[32,2048]{1,0:T(8,128)(2,1)S(1)} %node.9), channel_id=1, source_target_pairs={{0,56},{1,9},{2,58},{3,11},{4,60},{5,13},{6,62},{7,15},{8,0},{9,17... | collective-permute-start | bytes 393224 | tf_op jit(solution)/shard_map/ppermute | solution.py:164
  129.8 9.9 %collective-permute-start.28 = (bf16[16,2048]{1,0:T(8,128)(2,1)S(1)}, bf16[16,2048]{1,0:T(8,128)(2,1)S(1)}, u32[]{:S(2)}, u32[]{:S(2)}) collective-permute-start(bf16[16,2048]{1,0:T(8,128)(2,1)S(1)} %get-tuple-element.45), channel_id=1, source_target_pairs={{0,62},{1,3},{2,0},{3,5},{4,2},{5,7},{6,4},{7,9},{8,6},{9,11},{10,... | collective-permute-start | bytes 196616 | tf_op jit(solution)/shard_map/ppermute | solution.py:164
  135.9 21.5 %collective-permute-start.34 = (bf16[32,2048]{1,0:T(8,128)(2,1)S(1)}, bf16[32,2048]{1,0:T(8,128)(2,1)S(1)}, u32[]{:S(2)}, u32[]{:S(2)}) collective-permute-start(bf16[32,2048]{1,0:T(8,128)(2,1)S(1)} %node.12), channel_id=1, source_target_pairs={{0,62},{1,3},{2,0},{3,5},{4,2},{5,7},{6,4},{7,9},{8,6},{9,11},{10,... | collective-permute-start | bytes 393224 | tf_op jit(solution)/shard_map/ppermute | solution.py:164
  139.8 19.6 %collective-permute-start.29 = (bf16[32,2048]{1,0:T(8,128)(2,1)S(1)}, bf16[32,2048]{1,0:T(8,128)(2,1)S(1)}, u32[]{:S(2)}, u32[]{:S(2)}) collective-permute-start(bf16[32,2048]{1,0:T(8,128)(2,1)S(1)} %node.10), channel_id=1, source_target_pairs={{0,50},{1,15},{2,52},{3,17},{4,54},{5,19},{6,56},{7,21},{8,58},{9,... | collective-permute-start | bytes 393224 | tf_op jit(solution)/shard_map/ppermute | solution.py:164
  143.4 14.0 %collective-permute-start.19 = (bf16[16,2048]{1,0:T(8,128)(2,1)S(1)}, bf16[16,2048]{1,0:T(8,128)(2,1)S(1)}, u32[]{:S(2)}, u32[]{:S(2)}) collective-permute-start(bf16[16,2048]{1,0:T(8,128)(2,1)S(1)} %get-tuple-element.35), channel_id=1, source_target_pairs={{0,58},{1,7},{2,60},{3,9},{4,62},{5,11},{6,0},{7,13},{8,2},{9,15},... | collective-permute-start | bytes 196616 | tf_op jit(solution)/shard_map/ppermute | solution.py:164
  (17 other events, 122.6 us)

commit v2 on v1

--- a/solution.py
+++ b/solution.py
@@ -122,6 +122,21 @@
     )(tokens, norm_gain[None, :], group_prob[None, :], route_logits.T, expert_ids.T)
 
 
+def hold_kernel(source, out):
+    out[...] = source[...]
+
+
+def hold(array):
+    return pl.pallas_call(
+        hold_kernel,
+        out_shape=jax.ShapeDtypeStruct(array.shape, array.dtype),
+        in_specs=[VMEM],
+        out_specs=VMEM,
+        compiler_params=pltpu.CompilerParams(vmem_limit_bytes=8 * 1024 * 1024),
+        name="hold",
+    )(array)
+
+
 def expert(units, own, other):
     n = len(units)
     half, width = units[0].shape
@@ -211,7 +226,9 @@
     parts = {at: [(out, 0)] for at, out in enumerate(outs)}
     for at in COMBINE_ORDER:
         by = COMBINE[at - 1]
-        sent = added(parts[at]) if at in COMBINE else outs[at]
+        sent = outs[at]
+        if at in COMBINE:
+            sent = added(parts[at])
         came = turned(sent, by - at)
         parts[by].append((came, None if at in COMBINE else at - by))
     return added(parts[0])
@@ -223,6 +240,7 @@
         other.append(swapped(w))
     unit, kept, back = prepare(tokens, norm_gain, group_prob, route_logits, expert_ids)
     units = gather(unit)
+    kept = hold(kept)
     mixed = combine(expert([kept, *units[1:]], own, other))
     return finish(mixed, swapped(mixed), back)
 

time: 162 us -> 161 us (level)
  the two profiles are of different devices: /device:TPU:38 before, /device:TPU:173 now
where the time goes in v2:
time: 161 us
  starting transfers between devices  108 us (67%)
  waiting for transfers between devices  46.8 us (29%)
  Pallas kernels  5.02 us (3%)
    ppermute x32, starting transfers between devices, turned(): return lax.ppermute(array, ('ep', 'tp'), pairs)  84.2 us
    ppermute x32, waiting for transfers between devices, turned(): return lax.ppermute(array, ('ep', 'tp'), pairs)  45.8 us
    ppermute x4, starting transfers between devices, swapped(): return lax.ppermute(array, 'tp', [(0, 1), (1, 0)])  23.3 us
  transfers between devices with their start and end apart: 36, of which 21 were waited for; matrix products, arithmetic and copies ran while one was open for 0% of the time, Pallas kernels for 0%

profile of v2, /device:TPU:173, one launch (start us, length us, event | category | flops | bytes accessed | tf_op | source)
XLA Modules:
  0.0 161.2 jit_solution(8139970858480141139)
XLA Ops:
  1.9 24.3 %collective-permute-start.5 = (bf16[32,2176]{1,0:T(8,128)(2,1)}, bf16[32,2176]{1,0:T(8,128)(2,1)S(1)}, u32[]{:S(2)}, u32[]{:S(2)}) collective-permute-start(bf16[32,2176]{1,0:T(8,128)(2,1)} %get-tuple-element.30), channel_id=1, source_target_pairs={{0,12},{1,53},{2,14},{3,55},{4,16},{5,57},{6,18},{7,59},{8,20},{9,... | collective-permute-start | bytes 417800 | tf_op jit(solution)/shard_map/ppermute | solution.py:179
  27.7 8.8 %collective-permute-done.5.refs_6_ = bf16[32,2176]{1,0:T(8,128)(2,1)S(1)} collective-permute-done((bf16[32,2176]{1,0:T(8,128)(2,1)}, bf16[32,2176]{1,0:T(8,128)(2,1)S(1)}, u32[]{:S(2)}, u32[]{:S(2)}) %collective-permute-start.5) | collective-permute-done | bytes 139296 | tf_op jit(solution)/shard_map/ppermute | solution.py:179
  38.5 7.1 %collective-permute-start.9 = (bf16[32,2176]{1,0:T(8,128)(2,1)S(1)}, bf16[32,2176]{1,0:T(8,128)(2,1)S(1)}, u32[]{:S(2)}, u32[]{:S(2)}) collective-permute-start(bf16[32,2176]{1,0:T(8,128)(2,1)S(1)} %collective-permute-done.5.refs_6_), channel_id=1, source_target_pairs={{0,8},{1,57},{2,10},{3,59},{4,12},{5,61},{6,14},{7,63},{8,16},{9,1... | collective-permute-start | bytes 417800 | tf_op jit(solution)/shard_map/ppermute | solution.py:179
  46.2 2.3 %collective-permute-done.9.refs_10_ = bf16[32,2176]{1,0:T(8,128)(2,1)S(1)} collective-permute-done((bf16[32,2176]{1,0:T(8,128)(2,1)S(1)}, bf16[32,2176]{1,0:T(8,128)(2,1)S(1)}, u32[]{:S(2)}, u32[]{:S(2)}) %collective-permute-start.9) | collective-permute-done | bytes 139296 | tf_op jit(solution)/shard_map/ppermute | solution.py:179
  48.5 4.5 %collective-permute-start.6 = (bf16[32,2176]{1,0:T(8,128)(2,1)S(1)}, bf16[32,2176]{1,0:T(8,128)(2,1)S(1)}, u32[]{:S(2)}, u32[]{:S(2)}) collective-permute-start(bf16[32,2176]{1,0:T(8,128)(2,1)S(1)} %collective-permute-done.5.refs_6_), channel_id=1, source_target_pairs={{0,2},{1,63},{2,4},{3,1},{4,6},{5,3},{6,8},{7,5},{8,10},{9,7},{10,... | collective-permute-start | bytes 417800 | tf_op jit(solution)/shard_map/ppermute | solution.py:179
  55.1 2.1 %collective-permute-start.1 = (bf16[32,2176]{1,0:T(8,128)(2,1)S(1)}, bf16[32,2176]{1,0:T(8,128)(2,1)S(1)}, u32[]{:S(2)}, u32[]{:S(2)}) collective-permute-start(bf16[32,2176]{1,0:T(8,128)(2,1)S(1)} %collective-permute-done.refs_1_), channel_id=1, source_target_pairs={{0,2},{1,63},{2,4},{3,1},{4,6},{5,3},{6,8},{7,5},{8,10},{9,7},{10,... | collective-permute-start | bytes 417800 | tf_op jit(solution)/shard_map/ppermute | solution.py:179
  58.0 3.3 %collective-permute-start.12 = (bf16[32,2176]{1,0:T(8,128)(2,1)S(1)}, bf16[32,2176]{1,0:T(8,128)(2,1)S(1)}, u32[]{:S(2)}, u32[]{:S(2)}) collective-permute-start(bf16[32,2176]{1,0:T(8,128)(2,1)S(1)} %collective-permute-done.9.refs_10_), channel_id=1, source_target_pairs={{0,6},{1,59},{2,8},{3,61},{4,10},{5,63},{6,12},{7,1},{8,14},{9,3},... | collective-permute-start | bytes 417800 | tf_op jit(solution)/shard_map/ppermute | solution.py:179
  63.0 4.9 %collective-permute-done.12.refs_13_ = bf16[32,2176]{1,0:T(8,128)(2,1)S(1)} collective-permute-done((bf16[32,2176]{1,0:T(8,128)(2,1)S(1)}, bf16[32,2176]{1,0:T(8,128)(2,1)S(1)}, u32[]{:S(2)}, u32[]{:S(2)}) %collective-permute-start.12) | collective-permute-done | bytes 139296 | tf_op jit(solution)/shard_map/ppermute | solution.py:179
  68.5 2.0 %collective-permute-start.4 = (bf16[32,2176]{1,0:T(8,128)(2,1)S(1)}, bf16[32,2176]{1,0:T(8,128)(2,1)S(1)}, u32[]{:S(2)}, u32[]{:S(2)}) collective-permute-start(bf16[32,2176]{1,0:T(8,128)(2,1)S(1)} %collective-permute-done.3.refs_4_), channel_id=1, source_target_pairs={{0,2},{1,63},{2,4},{3,1},{4,6},{5,3},{6,8},{7,5},{8,10},{9,7},{10,... | collective-permute-start | bytes 417800 | tf_op jit(solution)/shard_map/ppermute | solution.py:179
  72.1 3.2 %collective-permute-start.14 = (bf16[32,2176]{1,0:T(8,128)(2,1)S(1)}, bf16[32,2176]{1,0:T(8,128)(2,1)S(1)}, u32[]{:S(2)}, u32[]{:S(2)}) collective-permute-start(bf16[32,2176]{1,0:T(8,128)(2,1)S(1)} %collective-permute-done.12.refs_13_), channel_id=1, source_target_pairs={{0,4},{1,61},{2,6},{3,63},{4,8},{5,1},{6,10},{7,3},{8,12},{9,5},{1... | collective-permute-start | bytes 417800 | tf_op jit(solution)/shard_map/ppermute | solution.py:179
  75.5 2.3 %collective-permute-done.14.refs_15_ = bf16[32,2176]{1,0:T(8,128)(2,1)S(1)} collective-permute-done((bf16[32,2176]{1,0:T(8,128)(2,1)S(1)}, bf16[32,2176]{1,0:T(8,128)(2,1)S(1)}, u32[]{:S(2)}, u32[]{:S(2)}) %collective-permute-start.14) | collective-permute-done | bytes 139296 | tf_op jit(solution)/shard_map/ppermute | solution.py:179
  79.5 2.6 %collective-permute-start.15 = (bf16[32,2176]{1,0:T(8,128)(2,1)S(1)}, bf16[32,2176]{1,0:T(8,128)(2,1)S(1)}, u32[]{:S(2)}, u32[]{:S(2)}) collective-permute-start(bf16[32,2176]{1,0:T(8,128)(2,1)S(1)} %collective-permute-done.14.refs_15_), channel_id=1, source_target_pairs={{0,2},{1,63},{2,4},{3,1},{4,6},{5,3},{6,8},{7,5},{8,10},{9,7},{10,... | collective-permute-start | bytes 417800 | tf_op jit(solution)/shard_map/ppermute | solution.py:179
  86.7 2.0 %collective-permute-start.23 = (bf16[16,2048]{1,0:T(8,128)(2,1)S(1)}, bf16[16,2048]{1,0:T(8,128)(2,1)S(1)}, u32[]{:S(2)}, u32[]{:S(2)}) collective-permute-start(bf16[16,2048]{1,0:T(8,128)(2,1)S(1)} %get-tuple-element.42), channel_id=1, source_target_pairs={{0,60},{1,5},{2,62},{3,7},{4,0},{5,9},{6,2},{7,11},{8,4},{9,13},{1... | collective-permute-start | bytes 196616 | tf_op jit(solution)/shard_map/ppermute | solution.py:179
  89.0 4.0 %collective-permute-done.23.refs_1_ = bf16[16,2048]{1,0:T(8,128)(2,1)S(1)} collective-permute-done((bf16[16,2048]{1,0:T(8,128)(2,1)S(1)}, bf16[16,2048]{1,0:T(8,128)(2,1)S(1)}, u32[]{:S(2)}, u32[]{:S(2)}) %collective-permute-start.23) | collective-permute-done | bytes 65568 | tf_op jit(solution)/shard_map/ppermute | solution.py:179
  99.9 3.0 %collective-permute-start.32 = (bf16[32,2048]{1,0:T(8,128)(2,1)S(1)}, bf16[32,2048]{1,0:T(8,128)(2,1)S(1)}, u32[]{:S(2)}, u32[]{:S(2)}) collective-permute-start(bf16[32,2048]{1,0:T(8,128)(2,1)S(1)} %node.11), channel_id=1, source_target_pairs={{0,58},{1,7},{2,60},{3,9},{4,62},{5,11},{6,0},{7,13},{8,2},{9,15},... | collective-permute-start | bytes 393224 | tf_op jit(solution)/shard_map/ppermute | solution.py:179
  104.3 2.1 %collective-permute-done.22.refs_1_ = bf16[16,2048]{1,0:T(8,128)(2,1)S(1)} collective-permute-done((bf16[16,2048]{1,0:T(8,128)(2,1)S(1)}, bf16[16,2048]{1,0:T(8,128)(2,1)S(1)}, u32[]{:S(2)}, u32[]{:S(2)}) %collective-permute-start.22) | collective-permute-done | bytes 65568 | tf_op jit(solution)/shard_map/ppermute | solution.py:179
  106.6 3.1 %collective-permute-start.27 = (bf16[32,2048]{1,0:T(8,128)(2,1)S(1)}, bf16[32,2048]{1,0:T(8,128)(2,1)S(1)}, u32[]{:S(2)}, u32[]{:S(2)}) collective-permute-start(bf16[32,2048]{1,0:T(8,128)(2,1)S(1)} %node.9), channel_id=1, source_target_pairs={{0,56},{1,9},{2,58},{3,11},{4,60},{5,13},{6,62},{7,15},{8,0},{9,17... | collective-permute-start | bytes 393224 | tf_op jit(solution)/shard_map/ppermute | solution.py:179
  110.1 3.3 %collective-permute-start.28 = (bf16[16,2048]{1,0:T(8,128)(2,1)S(1)}, bf16[16,2048]{1,0:T(8,128)(2,1)S(1)}, u32[]{:S(2)}, u32[]{:S(2)}) collective-permute-start(bf16[16,2048]{1,0:T(8,128)(2,1)S(1)} %get-tuple-element.45), channel_id=1, source_target_pairs={{0,62},{1,3},{2,0},{3,5},{4,2},{5,7},{6,4},{7,9},{8,6},{9,11},{10,... | collective-permute-start | bytes 196616 | tf_op jit(solution)/shard_map/ppermute | solution.py:179
  113.4 2.5 %collective-permute-done.33.refs_2_ = bf16[16,2048]{1,0:T(8,128)(2,1)S(1)} collective-permute-done((bf16[16,2048]{1,0:T(8,128)(2,1)S(1)}, bf16[16,2048]{1,0:T(8,128)(2,1)S(1)}, u32[]{:S(2)}, u32[]{:S(2)}) %collective-permute-start.33) | collective-permute-done | bytes 65568 | tf_op jit(solution)/shard_map/ppermute | solution.py:179
  115.9 2.2 %collective-permute-start.34 = (bf16[32,2048]{1,0:T(8,128)(2,1)S(1)}, bf16[32,2048]{1,0:T(8,128)(2,1)S(1)}, u32[]{:S(2)}, u32[]{:S(2)}) collective-permute-start(bf16[32,2048]{1,0:T(8,128)(2,1)S(1)} %node.12), channel_id=1, source_target_pairs={{0,62},{1,3},{2,0},{3,5},{4,2},{5,7},{6,4},{7,9},{8,6},{9,11},{10,... | collective-permute-start | bytes 393224 | tf_op jit(solution)/shard_map/ppermute | solution.py:179
  119.2 7.8 %collective-permute-start.29 = (bf16[32,2048]{1,0:T(8,128)(2,1)S(1)}, bf16[32,2048]{1,0:T(8,128)(2,1)S(1)}, u32[]{:S(2)}, u32[]{:S(2)}) collective-permute-start(bf16[32,2048]{1,0:T(8,128)(2,1)S(1)} %node.10), channel_id=1, source_target_pairs={{0,50},{1,15},{2,52},{3,17},{4,54},{5,19},{6,56},{7,21},{8,58},{9,... | collective-permute-start | bytes 393224 | tf_op jit(solution)/shard_map/ppermute | solution.py:179
  126.9 3.2 %collective-permute-start.19 = (bf16[16,2048]{1,0:T(8,128)(2,1)S(1)}, bf16[16,2048]{1,0:T(8,128)(2,1)S(1)}, u32[]{:S(2)}, u32[]{:S(2)}) collective-permute-start(bf16[16,2048]{1,0:T(8,128)(2,1)S(1)} %get-tuple-element.35), channel_id=1, source_target_pairs={{0,58},{1,7},{2,60},{3,9},{4,62},{5,11},{6,0},{7,13},{8,2},{9,15},... | collective-permute-start | bytes 196616 | tf_op jit(solution)/shard_map/ppermute | solution.py:179
  130.1 6.4 %collective-permute-done.19.refs_1_ = bf16[16,2048]{1,0:T(8,128)(2,1)S(1)} collective-permute-done((bf16[16,2048]{1,0:T(8,128)(2,1)S(1)}, bf16[16,2048]{1,0:T(8,128)(2,1)S(1)}, u32[]{:S(2)}, u32[]{:S(2)}) %collective-permute-start.19) | collective-permute-done | bytes 65568 | tf_op jit(solution)/shard_map/ppermute | solution.py:179
  136.6 22.8 %collective-permute-start.35 = (bf16[32,2048]{1,0:T(8,128)(2,1)S(1)}, bf16[32,2048]{1,0:T(8,128)(2,1)S(1)}, u32[]{:S(2)}, u32[]{:S(2)}) collective-permute-start(bf16[32,2048]{1,0:T(8,128)(2,1)S(1)} %node.13), channel_id=1, source_target_pairs={{0,1},{1,0},{2,3},{3,2},{4,5},{5,4},{6,7},{7,6},{8,9},{9,8},{10,11... | collective-permute-start | bytes 393224 | tf_op jit(solution)/shard_map/ppermute | solution.py:183
  (70 shorter events, 31.5 us)
Async XLA Ops:
  1.9 34.6 %collective-permute-start.5 = (bf16[32,2176]{1,0:T(8,128)(2,1)}, bf16[32,2176]{1,0:T(8,128)(2,1)S(1)}, u32[]{:S(2)}, u32[]{:S(2)}) collective-permute-start(bf16[32,2176]{1,0:T(8,128)(2,1)} %get-tuple-element.30), channel_id=1, source_target_pairs={{0,12},{1,53},{2,14},{3,55},{4,16},{5,57},{6,18},{7,59},{8,20},{9,... | collective-permute-start | bytes 417800 | tf_op jit(solution)/shard_map/ppermute | solution.py:179
  26.2 12.3 %collective-permute-start.2 = (bf16[32,2176]{1,0:T(8,128)(2,1)}, bf16[32,2176]{1,0:T(8,128)(2,1)S(1)}, u32[]{:S(2)}, u32[]{:S(2)}) collective-permute-start(bf16[32,2176]{1,0:T(8,128)(2,1)} %get-tuple-element.30), channel_id=1, source_target_pairs={{0,6},{1,59},{2,8},{3,61},{4,10},{5,63},{6,12},{7,1},{8,14},{9,3},... | collective-permute-start | bytes 417800 | tf_op jit(solution)/shard_map/ppermute | solution.py:179
  27.2 56.9 %collective-permute-start.16 = (bf16[1,2048,256]{2,1,0:T(8,128)(2,1)}, bf16[1,2048,256]{2,1,0:T(8,128)(2,1)S(1)}, u32[]{:S(2)}, u32[]{:S(2)}) collective-permute-start(bf16[1,2048,256]{2,1,0:T(8,128)(2,1)} %refs_3_.1), channel_id=1, source_target_pairs={{0,1},{1,0},{2,3},{3,2},{4,5},{5,4},{6,7},{7,6},{8,9},{9,8},{10,11... | collective-permute-start | bytes 3145736 | tf_op jit(solution)/shard_map/ppermute | solution.py:183
  27.2 56.9 %collective-permute-start.17 = (bf16[1,2048,256]{2,1,0:T(8,128)(2,1)}, bf16[1,2048,256]{2,1,0:T(8,128)(2,1)S(1)}, u32[]{:S(2)}, u32[]{:S(2)}) collective-permute-start(bf16[1,2048,256]{2,1,0:T(8,128)(2,1)} %refs_4_.1), channel_id=1, source_target_pairs={{0,1},{1,0},{2,3},{3,2},{4,5},{5,4},{6,7},{7,6},{8,9},{9,8},{10,11... | collective-permute-start | bytes 3145736 | tf_op jit(solution)/shard_map/ppermute | solution.py:183
  27.7 56.4 %collective-permute-start.18 = (bf16[1,256,2048]{2,1,0:T(8,128)(2,1)}, bf16[1,256,2048]{2,1,0:T(8,128)(2,1)S(1)}, u32[]{:S(2)}, u32[]{:S(2)}) collective-permute-start(bf16[1,256,2048]{2,1,0:T(8,128)(2,1)} %refs_5_.1), channel_id=1, source_target_pairs={{0,1},{1,0},{2,3},{3,2},{4,5},{5,4},{6,7},{7,6},{8,9},{9,8},{10,11... | collective-permute-start | bytes 3145736 | tf_op jit(solution)/shard_map/ppermute | solution.py:183
  36.5 9.0 %collective-permute-start = (bf16[32,2176]{1,0:T(8,128)(2,1)}, bf16[32,2176]{1,0:T(8,128)(2,1)S(1)}, u32[]{:S(2)}, u32[]{:S(2)}) collective-permute-start(bf16[32,2176]{1,0:T(8,128)(2,1)} %get-tuple-element.30), channel_id=1, source_target_pairs={{0,2},{1,63},{2,4},{3,1},{4,6},{5,3},{6,8},{7,5},{8,10},{9,7},{10,... | collective-permute-start | bytes 417800 | tf_op jit(solution)/shard_map/ppermute | solution.py:179
  38.5 10.1 %collective-permute-start.9 = (bf16[32,2176]{1,0:T(8,128)(2,1)S(1)}, bf16[32,2176]{1,0:T(8,128)(2,1)S(1)}, u32[]{:S(2)}, u32[]{:S(2)}) collective-permute-start(bf16[32,2176]{1,0:T(8,128)(2,1)S(1)} %collective-permute-done.5.refs_6_), channel_id=1, source_target_pairs={{0,8},{1,57},{2,10},{3,59},{4,12},{5,61},{6,14},{7,63},{8,16},{9,1... | collective-permute-start | bytes 417800 | tf_op jit(solution)/shard_map/ppermute | solution.py:179
  45.5 8.3 %collective-permute-start.7 = (bf16[32,2176]{1,0:T(8,128)(2,1)S(1)}, bf16[32,2176]{1,0:T(8,128)(2,1)S(1)}, u32[]{:S(2)}, u32[]{:S(2)}) collective-permute-start(bf16[32,2176]{1,0:T(8,128)(2,1)S(1)} %collective-permute-done.5.refs_6_), channel_id=1, source_target_pairs={{0,4},{1,61},{2,6},{3,63},{4,8},{5,1},{6,10},{7,3},{8,12},{9,5},{1... | collective-permute-start | bytes 417800 | tf_op jit(solution)/shard_map/ppermute | solution.py:179
  58.0 9.9 %collective-permute-start.12 = (bf16[32,2176]{1,0:T(8,128)(2,1)S(1)}, bf16[32,2176]{1,0:T(8,128)(2,1)S(1)}, u32[]{:S(2)}, u32[]{:S(2)}) collective-permute-start(bf16[32,2176]{1,0:T(8,128)(2,1)S(1)} %collective-permute-done.9.refs_10_), channel_id=1, source_target_pairs={{0,6},{1,59},{2,8},{3,61},{4,10},{5,63},{6,12},{7,1},{8,14},{9,3},... | collective-permute-start | bytes 417800 | tf_op jit(solution)/shard_map/ppermute | solution.py:179
  61.3 7.2 %collective-permute-start.10 = (bf16[32,2176]{1,0:T(8,128)(2,1)S(1)}, bf16[32,2176]{1,0:T(8,128)(2,1)S(1)}, u32[]{:S(2)}, u32[]{:S(2)}) collective-permute-start(bf16[32,2176]{1,0:T(8,128)(2,1)S(1)} %collective-permute-done.9.refs_10_), channel_id=1, source_target_pairs={{0,2},{1,63},{2,4},{3,1},{4,6},{5,3},{6,8},{7,5},{8,10},{9,7},{10,... | collective-permute-start | bytes 417800 | tf_op jit(solution)/shard_map/ppermute | solution.py:179
  68.5 6.8 %collective-permute-start.4 = (bf16[32,2176]{1,0:T(8,128)(2,1)S(1)}, bf16[32,2176]{1,0:T(8,128)(2,1)S(1)}, u32[]{:S(2)}, u32[]{:S(2)}) collective-permute-start(bf16[32,2176]{1,0:T(8,128)(2,1)S(1)} %collective-permute-done.3.refs_4_), channel_id=1, source_target_pairs={{0,2},{1,63},{2,4},{3,1},{4,6},{5,3},{6,8},{7,5},{8,10},{9,7},{10,... | collective-permute-start | bytes 417800 | tf_op jit(solution)/shard_map/ppermute | solution.py:179
  88.7 8.4 %collective-permute-start.30 = (bf16[16,2048]{1,0:T(8,128)(2,1)S(1)}, bf16[16,2048]{1,0:T(8,128)(2,1)S(1)}, u32[]{:S(2)}, u32[]{:S(2)}) collective-permute-start(bf16[16,2048]{1,0:T(8,128)(2,1)S(1)} %get-tuple-element.48), channel_id=1, source_target_pairs={{0,60},{1,5},{2,62},{3,7},{4,0},{5,9},{6,2},{7,11},{8,4},{9,13},{1... | collective-permute-start | bytes 196616 | tf_op jit(solution)/shard_map/ppermute | solution.py:179
  93.9 12.5 %collective-permute-start.25 = (bf16[32,2048]{1,0:T(8,128)(2,1)S(1)}, bf16[32,2048]{1,0:T(8,128)(2,1)S(1)}, u32[]{:S(2)}, u32[]{:S(2)}) collective-permute-start(bf16[32,2048]{1,0:T(8,128)(2,1)S(1)} %node.8), channel_id=1, source_target_pairs={{0,58},{1,7},{2,60},{3,9},{4,62},{5,11},{6,0},{7,13},{8,2},{9,15},... | collective-permute-start | bytes 393224 | tf_op jit(solution)/shard_map/ppermute | solution.py:179
  95.5 7.3 %collective-permute-start.20 = (bf16[16,2048]{1,0:T(8,128)(2,1)S(1)}, bf16[16,2048]{1,0:T(8,128)(2,1)S(1)}, u32[]{:S(2)}, u32[]{:S(2)}) collective-permute-start(bf16[16,2048]{1,0:T(8,128)(2,1)S(1)} %get-tuple-element.38), channel_id=1, source_target_pairs={{0,62},{1,3},{2,0},{3,5},{4,2},{5,7},{6,4},{7,9},{8,6},{9,11},{10,... | collective-permute-start | bytes 196616 | tf_op jit(solution)/shard_map/ppermute | solution.py:179
  95.5 11.0 %collective-permute-start.22 = (bf16[16,2048]{1,0:T(8,128)(2,1)S(1)}, bf16[16,2048]{1,0:T(8,128)(2,1)S(1)}, u32[]{:S(2)}, u32[]{:S(2)}) collective-permute-start(bf16[16,2048]{1,0:T(8,128)(2,1)S(1)} %get-tuple-element.40), channel_id=1, source_target_pairs={{0,60},{1,5},{2,62},{3,7},{4,0},{5,9},{6,2},{7,11},{8,4},{9,13},{1... | collective-permute-start | bytes 196616 | tf_op jit(solution)/shard_map/ppermute | solution.py:179
  97.2 9.3 %collective-permute-start.26 = (bf16[16,2048]{1,0:T(8,128)(2,1)S(1)}, bf16[16,2048]{1,0:T(8,128)(2,1)S(1)}, u32[]{:S(2)}, u32[]{:S(2)}) collective-permute-start(bf16[16,2048]{1,0:T(8,128)(2,1)S(1)} %get-tuple-element.44), channel_id=1, source_target_pairs={{0,62},{1,3},{2,0},{3,5},{4,2},{5,7},{6,4},{7,9},{8,6},{9,11},{10,... | collective-permute-start | bytes 196616 | tf_op jit(solution)/shard_map/ppermute | solution.py:179
  99.9 16.0 %collective-permute-start.32 = (bf16[32,2048]{1,0:T(8,128)(2,1)S(1)}, bf16[32,2048]{1,0:T(8,128)(2,1)S(1)}, u32[]{:S(2)}, u32[]{:S(2)}) collective-permute-start(bf16[32,2048]{1,0:T(8,128)(2,1)S(1)} %node.11), channel_id=1, source_target_pairs={{0,58},{1,7},{2,60},{3,9},{4,62},{5,11},{6,0},{7,13},{8,2},{9,15},... | collective-permute-start | bytes 393224 | tf_op jit(solution)/shard_map/ppermute | solution.py:179
  102.9 15.3 %collective-permute-start.21 = (bf16[32,2048]{1,0:T(8,128)(2,1)S(1)}, bf16[32,2048]{1,0:T(8,128)(2,1)S(1)}, u32[]{:S(2)}, u32[]{:S(2)}) collective-permute-start(bf16[32,2048]{1,0:T(8,128)(2,1)S(1)} %node.7), channel_id=1, source_target_pairs={{0,60},{1,5},{2,62},{3,7},{4,0},{5,9},{6,2},{7,11},{8,4},{9,13},{1... | collective-permute-start | bytes 393224 | tf_op jit(solution)/shard_map/ppermute | solution.py:179
  106.6 12.5 %collective-permute-start.27 = (bf16[32,2048]{1,0:T(8,128)(2,1)S(1)}, bf16[32,2048]{1,0:T(8,128)(2,1)S(1)}, u32[]{:S(2)}, u32[]{:S(2)}) collective-permute-start(bf16[32,2048]{1,0:T(8,128)(2,1)S(1)} %node.9), channel_id=1, source_target_pairs={{0,56},{1,9},{2,58},{3,11},{4,60},{5,13},{6,62},{7,15},{8,0},{9,17... | collective-permute-start | bytes 393224 | tf_op jit(solution)/shard_map/ppermute | solution.py:179
  110.1 8.1 %collective-permute-start.28 = (bf16[16,2048]{1,0:T(8,128)(2,1)S(1)}, bf16[16,2048]{1,0:T(8,128)(2,1)S(1)}, u32[]{:S(2)}, u32[]{:S(2)}) collective-permute-start(bf16[16,2048]{1,0:T(8,128)(2,1)S(1)} %get-tuple-element.45), channel_id=1, source_target_pairs={{0,62},{1,3},{2,0},{3,5},{4,2},{5,7},{6,4},{7,9},{8,6},{9,11},{10,... | collective-permute-start | bytes 196616 | tf_op jit(solution)/shard_map/ppermute | solution.py:179
  115.9 20.6 %collective-permute-start.34 = (bf16[32,2048]{1,0:T(8,128)(2,1)S(1)}, bf16[32,2048]{1,0:T(8,128)(2,1)S(1)}, u32[]{:S(2)}, u32[]{:S(2)}) collective-permute-start(bf16[32,2048]{1,0:T(8,128)(2,1)S(1)} %node.12), channel_id=1, source_target_pairs={{0,62},{1,3},{2,0},{3,5},{4,2},{5,7},{6,4},{7,9},{8,6},{9,11},{10,... | collective-permute-start | bytes 393224 | tf_op jit(solution)/shard_map/ppermute | solution.py:179
  119.2 17.4 %collective-permute-start.29 = (bf16[32,2048]{1,0:T(8,128)(2,1)S(1)}, bf16[32,2048]{1,0:T(8,128)(2,1)S(1)}, u32[]{:S(2)}, u32[]{:S(2)}) collective-permute-start(bf16[32,2048]{1,0:T(8,128)(2,1)S(1)} %node.10), channel_id=1, source_target_pairs={{0,50},{1,15},{2,52},{3,17},{4,54},{5,19},{6,56},{7,21},{8,58},{9,... | collective-permute-start | bytes 393224 | tf_op jit(solution)/shard_map/ppermute | solution.py:179
  126.9 9.6 %collective-permute-start.19 = (bf16[16,2048]{1,0:T(8,128)(2,1)S(1)}, bf16[16,2048]{1,0:T(8,128)(2,1)S(1)}, u32[]{:S(2)}, u32[]{:S(2)}) collective-permute-start(bf16[16,2048]{1,0:T(8,128)(2,1)S(1)} %get-tuple-element.35), channel_id=1, source_target_pairs={{0,58},{1,7},{2,60},{3,9},{4,62},{5,11},{6,0},{7,13},{8,2},{9,15},... | collective-permute-start | bytes 196616 | tf_op jit(solution)/shard_map/ppermute | solution.py:179
  136.6 23.8 %collective-permute-start.35 = (bf16[32,2048]{1,0:T(8,128)(2,1)S(1)}, bf16[32,2048]{1,0:T(8,128)(2,1)S(1)}, u32[]{:S(2)}, u32[]{:S(2)}) collective-permute-start(bf16[32,2048]{1,0:T(8,128)(2,1)S(1)} %node.13), channel_id=1, source_target_pairs={{0,1},{1,0},{2,3},{3,2},{4,5},{5,4},{6,7},{7,6},{8,9},{9,8},{10,11... | collective-permute-start | bytes 393224 | tf_op jit(solution)/shard_map/ppermute | solution.py:183
  (17 other events, 131.2 us)

commit v3 on v2

--- a/solution.py
+++ b/solution.py
@@ -10,10 +10,10 @@
 
 LANES = 128
 GROUPS = 2
-GATHER = (0, 1, 0, 3, 4, 0, 6, 6, 8, 6, 10, 11, 10, 13, 13, 15)
-GATHER_ORDER = (6, 1, 3, 10, 8, 4, 7, 13, 11, 5, 2, 15, 14, 12, 9, 16)
-COMBINE = (0, 1, 0, 1, 4, 4, 0, 7, 7, 9, 7, 11, 11, 11, 14, 14)
-COMBINE_ORDER = (16, 15, 13, 10, 14, 12, 9, 6, 5, 11, 8, 3, 4, 2, 7, 1)
+GATHER = (0, 0, 2, 0, 4, 4, 6, 7, 4, 9, 10, 9, 12, 12, 14, 14)
+GATHER_ORDER = (4, 1, 2, 9, 5, 6, 12, 10, 7, 3, 14, 11, 13, 8, 15, 16)
+COMBINE = (0, 0, 2, 3, 0, 5, 5, 7, 8, 5, 10, 11, 10, 13, 13, 15)
+COMBINE_ORDER = (16, 12, 9, 14, 15, 8, 4, 11, 1, 13, 6, 7, 3, 10, 2, 5)
 LAST = len(GATHER)
 
 

time: 161 us -> 159 us (0.988)
  the two profiles are of different devices: /device:TPU:173 before, /device:TPU:38 now
where the time goes in v3:
time: 159 us; the launch traced here: 158 us
  starting transfers between devices  79.3 us (50%)
  waiting for transfers between devices  71.2 us (45%)
  Pallas kernels  5.15 us (3%)
    ppermute x32, waiting for transfers between devices, turned(): return lax.ppermute(array, ('ep', 'tp'), pairs)  69.9 us
    ppermute x32, starting transfers between devices, turned(): return lax.ppermute(array, ('ep', 'tp'), pairs)  65 us
    ppermute x4, starting transfers between devices, swapped(): return lax.ppermute(array, 'tp', [(0, 1), (1, 0)])  14.3 us
  transfers between devices with their start and end apart: 36, of which 22 were waited for; matrix products, arithmetic and copies ran while one was open for 0% of the time, Pallas kernels for 0%

profile of v3, /device:TPU:38, one launch (start us, length us, event | category | flops | bytes accessed | tf_op | source)
XLA Modules:
  0.0 157.6 jit_solution(2742506280871128831)
XLA Ops:
  1.9 8.0 %collective-permute-start.3 = (bf16[32,2176]{1,0:T(8,128)(2,1)}, bf16[32,2176]{1,0:T(8,128)(2,1)S(1)}, u32[]{:S(2)}, u32[]{:S(2)}) collective-permute-start(bf16[32,2176]{1,0:T(8,128)(2,1)} %get-tuple-element.30), channel_id=1, source_target_pairs={{0,8},{1,57},{2,10},{3,59},{4,12},{5,61},{6,14},{7,63},{8,16},{9,1... | collective-permute-start | bytes 417800 | tf_op jit(solution)/shard_map/ppermute | solution.py:179
  9.9 3.7 %collective-permute-start.1 = (bf16[32,2176]{1,0:T(8,128)(2,1)}, bf16[32,2176]{1,0:T(8,128)(2,1)S(1)}, u32[]{:S(2)}, u32[]{:S(2)}) collective-permute-start(bf16[32,2176]{1,0:T(8,128)(2,1)} %get-tuple-element.30), channel_id=1, source_target_pairs={{0,4},{1,61},{2,6},{3,63},{4,8},{5,1},{6,10},{7,3},{8,12},{9,5},{1... | collective-permute-start | bytes 417800 | tf_op jit(solution)/shard_map/ppermute | solution.py:179
  13.6 13.7 %collective-permute-start.16 = (bf16[1,2048,256]{2,1,0:T(8,128)(2,1)}, bf16[1,2048,256]{2,1,0:T(8,128)(2,1)S(1)}, u32[]{:S(2)}, u32[]{:S(2)}) collective-permute-start(bf16[1,2048,256]{2,1,0:T(8,128)(2,1)} %refs_3_.1), channel_id=1, source_target_pairs={{0,1},{1,0},{2,3},{3,2},{4,5},{5,4},{6,7},{7,6},{8,9},{9,8},{10,11... | collective-permute-start | bytes 3145736 | tf_op jit(solution)/shard_map/ppermute | solution.py:183
  29.2 4.1 %collective-permute-start = (bf16[32,2176]{1,0:T(8,128)(2,1)}, bf16[32,2176]{1,0:T(8,128)(2,1)S(1)}, u32[]{:S(2)}, u32[]{:S(2)}) collective-permute-start(bf16[32,2176]{1,0:T(8,128)(2,1)} %get-tuple-element.30), channel_id=1, source_target_pairs={{0,2},{1,63},{2,4},{3,1},{4,6},{5,3},{6,8},{7,5},{8,10},{9,7},{10,... | collective-permute-start | bytes 417800 | tf_op jit(solution)/shard_map/ppermute | solution.py:179
  35.1 8.0 %collective-permute-done.refs_1_ = bf16[32,2176]{1,0:T(8,128)(2,1)S(1)} collective-permute-done((bf16[32,2176]{1,0:T(8,128)(2,1)}, bf16[32,2176]{1,0:T(8,128)(2,1)S(1)}, u32[]{:S(2)}, u32[]{:S(2)}) %collective-permute-start) | collective-permute-done | bytes 139296 | tf_op jit(solution)/shard_map/ppermute | solution.py:179
  43.2 4.1 %collective-permute-done.8.refs_9_ = bf16[32,2176]{1,0:T(8,128)(2,1)S(1)} collective-permute-done((bf16[32,2176]{1,0:T(8,128)(2,1)S(1)}, bf16[32,2176]{1,0:T(8,128)(2,1)S(1)}, u32[]{:S(2)}, u32[]{:S(2)}) %collective-permute-start.8) | collective-permute-done | bytes 139296 | tf_op jit(solution)/shard_map/ppermute | solution.py:179
  47.3 4.6 %collective-permute-start.4 = (bf16[32,2176]{1,0:T(8,128)(2,1)S(1)}, bf16[32,2176]{1,0:T(8,128)(2,1)S(1)}, u32[]{:S(2)}, u32[]{:S(2)}) collective-permute-start(bf16[32,2176]{1,0:T(8,128)(2,1)S(1)} %collective-permute-done.3.refs_4_), channel_id=1, source_target_pairs={{0,2},{1,63},{2,4},{3,1},{4,6},{5,3},{6,8},{7,5},{8,10},{9,7},{10,... | collective-permute-start | bytes 417800 | tf_op jit(solution)/shard_map/ppermute | solution.py:179
  53.7 3.0 %collective-permute-start.2 = (bf16[32,2176]{1,0:T(8,128)(2,1)S(1)}, bf16[32,2176]{1,0:T(8,128)(2,1)S(1)}, u32[]{:S(2)}, u32[]{:S(2)}) collective-permute-start(bf16[32,2176]{1,0:T(8,128)(2,1)S(1)} %collective-permute-done.1.refs_2_), channel_id=1, source_target_pairs={{0,2},{1,63},{2,4},{3,1},{4,6},{5,3},{6,8},{7,5},{8,10},{9,7},{10,... | collective-permute-start | bytes 417800 | tf_op jit(solution)/shard_map/ppermute | solution.py:179
  56.6 3.8 %collective-permute-start.11 = (bf16[32,2176]{1,0:T(8,128)(2,1)S(1)}, bf16[32,2176]{1,0:T(8,128)(2,1)S(1)}, u32[]{:S(2)}, u32[]{:S(2)}) collective-permute-start(bf16[32,2176]{1,0:T(8,128)(2,1)S(1)} %collective-permute-done.8.refs_9_), channel_id=1, source_target_pairs={{0,6},{1,59},{2,8},{3,61},{4,10},{5,63},{6,12},{7,1},{8,14},{9,3},... | collective-permute-start | bytes 417800 | tf_op jit(solution)/shard_map/ppermute | solution.py:179
  61.7 4.5 %collective-permute-done.11.refs_12_ = bf16[32,2176]{1,0:T(8,128)(2,1)S(1)} collective-permute-done((bf16[32,2176]{1,0:T(8,128)(2,1)S(1)}, bf16[32,2176]{1,0:T(8,128)(2,1)S(1)}, u32[]{:S(2)}, u32[]{:S(2)}) %collective-permute-start.11) | collective-permute-done | bytes 139296 | tf_op jit(solution)/shard_map/ppermute | solution.py:179
  70.6 4.1 %collective-permute-done.6.refs_7_ = bf16[32,2176]{1,0:T(8,128)(2,1)S(1)} collective-permute-done((bf16[32,2176]{1,0:T(8,128)(2,1)S(1)}, bf16[32,2176]{1,0:T(8,128)(2,1)S(1)}, u32[]{:S(2)}, u32[]{:S(2)}) %collective-permute-start.6) | collective-permute-done | bytes 139296 | tf_op jit(solution)/shard_map/ppermute | solution.py:179
  74.7 4.4 %collective-permute-done.13.refs_14_ = bf16[32,2176]{1,0:T(8,128)(2,1)S(1)} collective-permute-done((bf16[32,2176]{1,0:T(8,128)(2,1)S(1)}, bf16[32,2176]{1,0:T(8,128)(2,1)S(1)}, u32[]{:S(2)}, u32[]{:S(2)}) %collective-permute-start.13) | collective-permute-done | bytes 139296 | tf_op jit(solution)/shard_map/ppermute | solution.py:179
  81.0 4.4 %collective-permute-done.10.refs_11_ = bf16[32,2176]{1,0:T(8,128)(2,1)S(1)} collective-permute-done((bf16[32,2176]{1,0:T(8,128)(2,1)S(1)}, bf16[32,2176]{1,0:T(8,128)(2,1)S(1)}, u32[]{:S(2)}, u32[]{:S(2)}) %collective-permute-start.10) | collective-permute-done | bytes 139296 | tf_op jit(solution)/shard_map/ppermute | solution.py:179
  88.2 4.5 %collective-permute-done.15.refs_16_ = bf16[32,2176]{1,0:T(8,128)(2,1)S(1)} collective-permute-done((bf16[32,2176]{1,0:T(8,128)(2,1)S(1)}, bf16[32,2176]{1,0:T(8,128)(2,1)S(1)}, u32[]{:S(2)}, u32[]{:S(2)}) %collective-permute-start.15) | collective-permute-done | bytes 139296 | tf_op jit(solution)/shard_map/ppermute | solution.py:179
  97.5 4.2 %collective-permute-done.30.refs_1_ = bf16[16,2048]{1,0:T(8,128)(2,1)S(1)} collective-permute-done((bf16[16,2048]{1,0:T(8,128)(2,1)S(1)}, bf16[16,2048]{1,0:T(8,128)(2,1)S(1)}, u32[]{:S(2)}, u32[]{:S(2)}) %collective-permute-start.30) | collective-permute-done | bytes 65568 | tf_op jit(solution)/shard_map/ppermute | solution.py:179
  103.3 2.9 %collective-permute-start.27 = (bf16[16,2048]{1,0:T(8,128)(2,1)S(1)}, bf16[16,2048]{1,0:T(8,128)(2,1)S(1)}, u32[]{:S(2)}, u32[]{:S(2)}) collective-permute-start(bf16[16,2048]{1,0:T(8,128)(2,1)S(1)} %get-tuple-element.46), channel_id=1, source_target_pairs={{0,62},{1,3},{2,0},{3,5},{4,2},{5,7},{6,4},{7,9},{8,6},{9,11},{10,... | collective-permute-start | bytes 196616 | tf_op jit(solution)/shard_map/ppermute | solution.py:179
  114.3 3.2 %collective-permute-start.32 = (bf16[32,2048]{1,0:T(8,128)(2,1)S(1)}, bf16[32,2048]{1,0:T(8,128)(2,1)S(1)}, u32[]{:S(2)}, u32[]{:S(2)}) collective-permute-start(bf16[32,2048]{1,0:T(8,128)(2,1)S(1)} %node.16), channel_id=1, source_target_pairs={{0,58},{1,7},{2,60},{3,9},{4,62},{5,11},{6,0},{7,13},{8,2},{9,15},... | collective-permute-start | bytes 393224 | tf_op jit(solution)/shard_map/ppermute | solution.py:179
  118.0 6.8 %collective-permute-done.20.refs_1_ = bf16[16,2048]{1,0:T(8,128)(2,1)S(1)} collective-permute-done((bf16[16,2048]{1,0:T(8,128)(2,1)S(1)}, bf16[16,2048]{1,0:T(8,128)(2,1)S(1)}, u32[]{:S(2)}, u32[]{:S(2)}) %collective-permute-start.20) | collective-permute-done | bytes 65568 | tf_op jit(solution)/shard_map/ppermute | solution.py:179
  124.8 2.7 %collective-permute-start.21 = (bf16[32,2048]{1,0:T(8,128)(2,1)S(1)}, bf16[32,2048]{1,0:T(8,128)(2,1)S(1)}, u32[]{:S(2)}, u32[]{:S(2)}) collective-permute-start(bf16[32,2048]{1,0:T(8,128)(2,1)S(1)} %node.10), channel_id=1, source_target_pairs={{0,62},{1,3},{2,0},{3,5},{4,2},{5,7},{6,4},{7,9},{8,6},{9,11},{10,... | collective-permute-start | bytes 393224 | tf_op jit(solution)/shard_map/ppermute | solution.py:179
  127.9 3.2 %collective-permute-start.33 = (bf16[32,2048]{1,0:T(8,128)(2,1)S(1)}, bf16[32,2048]{1,0:T(8,128)(2,1)S(1)}, u32[]{:S(2)}, u32[]{:S(2)}) collective-permute-start(bf16[32,2048]{1,0:T(8,128)(2,1)S(1)} %node.17), channel_id=1, source_target_pairs={{0,54},{1,11},{2,56},{3,13},{4,58},{5,15},{6,60},{7,17},{8,62},{9,... | collective-permute-start | bytes 393224 | tf_op jit(solution)/shard_map/ppermute | solution.py:179
  134.2 7.6 %collective-permute-done.23.refs_1_ = bf16[16,2048]{1,0:T(8,128)(2,1)S(1)} collective-permute-done((bf16[16,2048]{1,0:T(8,128)(2,1)S(1)}, bf16[16,2048]{1,0:T(8,128)(2,1)S(1)}, u32[]{:S(2)}, u32[]{:S(2)}) %collective-permute-start.23) | collective-permute-done | bytes 65568 | tf_op jit(solution)/shard_map/ppermute | solution.py:179
  142.2 5.1 %collective-permute-start.34 = (bf16[32,2048]{1,0:T(8,128)(2,1)S(1)}, bf16[32,2048]{1,0:T(8,128)(2,1)S(1)}, u32[]{:S(2)}, u32[]{:S(2)}) collective-permute-start(bf16[32,2048]{1,0:T(8,128)(2,1)S(1)} %node.18), channel_id=1, source_target_pairs={{0,54},{1,11},{2,56},{3,13},{4,58},{5,15},{6,60},{7,17},{8,62},{9,... | collective-permute-start | bytes 393224 | tf_op jit(solution)/shard_map/ppermute | solution.py:179
  147.3 2.8 %collective-permute-start.19 = (bf16[16,2048]{1,0:T(8,128)(2,1)S(1)}, bf16[16,2048]{1,0:T(8,128)(2,1)S(1)}, u32[]{:S(2)}, u32[]{:S(2)}) collective-permute-start(bf16[16,2048]{1,0:T(8,128)(2,1)S(1)} %get-tuple-element.35), channel_id=1, source_target_pairs={{0,62},{1,3},{2,0},{3,5},{4,2},{5,7},{6,4},{7,9},{8,6},{9,11},{10,... | collective-permute-start | bytes 196616 | tf_op jit(solution)/shard_map/ppermute | solution.py:179
  150.1 2.9 %collective-permute-done.19.refs_1_ = bf16[16,2048]{1,0:T(8,128)(2,1)S(1)} collective-permute-done((bf16[16,2048]{1,0:T(8,128)(2,1)S(1)}, bf16[16,2048]{1,0:T(8,128)(2,1)S(1)}, u32[]{:S(2)}, u32[]{:S(2)}) %collective-permute-start.19) | collective-permute-done | bytes 65568 | tf_op jit(solution)/shard_map/ppermute | solution.py:179
  (73 shorter events, 41.0 us)
Async XLA Ops:
  1.9 27.3 %collective-permute-start.3 = (bf16[32,2176]{1,0:T(8,128)(2,1)}, bf16[32,2176]{1,0:T(8,128)(2,1)S(1)}, u32[]{:S(2)}, u32[]{:S(2)}) collective-permute-start(bf16[32,2176]{1,0:T(8,128)(2,1)} %get-tuple-element.30), channel_id=1, source_target_pairs={{0,8},{1,57},{2,10},{3,59},{4,12},{5,61},{6,14},{7,63},{8,16},{9,1... | collective-permute-start | bytes 417800 | tf_op jit(solution)/shard_map/ppermute | solution.py:179
  9.9 25.2 %collective-permute-start.1 = (bf16[32,2176]{1,0:T(8,128)(2,1)}, bf16[32,2176]{1,0:T(8,128)(2,1)S(1)}, u32[]{:S(2)}, u32[]{:S(2)}) collective-permute-start(bf16[32,2176]{1,0:T(8,128)(2,1)} %get-tuple-element.30), channel_id=1, source_target_pairs={{0,4},{1,61},{2,6},{3,63},{4,8},{5,1},{6,10},{7,3},{8,12},{9,5},{1... | collective-permute-start | bytes 417800 | tf_op jit(solution)/shard_map/ppermute | solution.py:179
  13.6 81.2 %collective-permute-start.16 = (bf16[1,2048,256]{2,1,0:T(8,128)(2,1)}, bf16[1,2048,256]{2,1,0:T(8,128)(2,1)S(1)}, u32[]{:S(2)}, u32[]{:S(2)}) collective-permute-start(bf16[1,2048,256]{2,1,0:T(8,128)(2,1)} %refs_3_.1), channel_id=1, source_target_pairs={{0,1},{1,0},{2,3},{3,2},{4,5},{5,4},{6,7},{7,6},{8,9},{9,8},{10,11... | collective-permute-start | bytes 3145736 | tf_op jit(solution)/shard_map/ppermute | solution.py:183
  27.3 67.5 %collective-permute-start.17 = (bf16[1,2048,256]{2,1,0:T(8,128)(2,1)}, bf16[1,2048,256]{2,1,0:T(8,128)(2,1)S(1)}, u32[]{:S(2)}, u32[]{:S(2)}) collective-permute-start(bf16[1,2048,256]{2,1,0:T(8,128)(2,1)} %refs_4_.1), channel_id=1, source_target_pairs={{0,1},{1,0},{2,3},{3,2},{4,5},{5,4},{6,7},{7,6},{8,9},{9,8},{10,11... | collective-permute-start | bytes 3145736 | tf_op jit(solution)/shard_map/ppermute | solution.py:183
  27.3 67.5 %collective-permute-start.18 = (bf16[1,256,2048]{2,1,0:T(8,128)(2,1)}, bf16[1,256,2048]{2,1,0:T(8,128)(2,1)S(1)}, u32[]{:S(2)}, u32[]{:S(2)}) collective-permute-start(bf16[1,256,2048]{2,1,0:T(8,128)(2,1)} %refs_5_.1), channel_id=1, source_target_pairs={{0,1},{1,0},{2,3},{3,2},{4,5},{5,4},{6,7},{7,6},{8,9},{9,8},{10,11... | collective-permute-start | bytes 3145736 | tf_op jit(solution)/shard_map/ppermute | solution.py:183
  29.2 13.9 %collective-permute-start = (bf16[32,2176]{1,0:T(8,128)(2,1)}, bf16[32,2176]{1,0:T(8,128)(2,1)S(1)}, u32[]{:S(2)}, u32[]{:S(2)}) collective-permute-start(bf16[32,2176]{1,0:T(8,128)(2,1)} %get-tuple-element.30), channel_id=1, source_target_pairs={{0,2},{1,63},{2,4},{3,1},{4,6},{5,3},{6,8},{7,5},{8,10},{9,7},{10,... | collective-permute-start | bytes 417800 | tf_op jit(solution)/shard_map/ppermute | solution.py:179
  35.1 12.2 %collective-permute-start.8 = (bf16[32,2176]{1,0:T(8,128)(2,1)S(1)}, bf16[32,2176]{1,0:T(8,128)(2,1)S(1)}, u32[]{:S(2)}, u32[]{:S(2)}) collective-permute-start(bf16[32,2176]{1,0:T(8,128)(2,1)S(1)} %collective-permute-done.3.refs_4_), channel_id=1, source_target_pairs={{0,10},{1,55},{2,12},{3,57},{4,14},{5,59},{6,16},{7,61},{8,18},{9,... | collective-permute-start | bytes 417800 | tf_op jit(solution)/shard_map/ppermute | solution.py:179
  43.2 10.5 %collective-permute-start.5 = (bf16[32,2176]{1,0:T(8,128)(2,1)S(1)}, bf16[32,2176]{1,0:T(8,128)(2,1)S(1)}, u32[]{:S(2)}, u32[]{:S(2)}) collective-permute-start(bf16[32,2176]{1,0:T(8,128)(2,1)S(1)} %collective-permute-done.3.refs_4_), channel_id=1, source_target_pairs={{0,4},{1,61},{2,6},{3,63},{4,8},{5,1},{6,10},{7,3},{8,12},{9,5},{1... | collective-permute-start | bytes 417800 | tf_op jit(solution)/shard_map/ppermute | solution.py:179
  47.3 9.4 %collective-permute-start.4 = (bf16[32,2176]{1,0:T(8,128)(2,1)S(1)}, bf16[32,2176]{1,0:T(8,128)(2,1)S(1)}, u32[]{:S(2)}, u32[]{:S(2)}) collective-permute-start(bf16[32,2176]{1,0:T(8,128)(2,1)S(1)} %collective-permute-done.3.refs_4_), channel_id=1, source_target_pairs={{0,2},{1,63},{2,4},{3,1},{4,6},{5,3},{6,8},{7,5},{8,10},{9,7},{10,... | collective-permute-start | bytes 417800 | tf_op jit(solution)/shard_map/ppermute | solution.py:179
  53.7 7.7 %collective-permute-start.2 = (bf16[32,2176]{1,0:T(8,128)(2,1)S(1)}, bf16[32,2176]{1,0:T(8,128)(2,1)S(1)}, u32[]{:S(2)}, u32[]{:S(2)}) collective-permute-start(bf16[32,2176]{1,0:T(8,128)(2,1)S(1)} %collective-permute-done.1.refs_2_), channel_id=1, source_target_pairs={{0,2},{1,63},{2,4},{3,1},{4,6},{5,3},{6,8},{7,5},{8,10},{9,7},{10,... | collective-permute-start | bytes 417800 | tf_op jit(solution)/shard_map/ppermute | solution.py:179
  56.6 9.5 %collective-permute-start.11 = (bf16[32,2176]{1,0:T(8,128)(2,1)S(1)}, bf16[32,2176]{1,0:T(8,128)(2,1)S(1)}, u32[]{:S(2)}, u32[]{:S(2)}) collective-permute-start(bf16[32,2176]{1,0:T(8,128)(2,1)S(1)} %collective-permute-done.8.refs_9_), channel_id=1, source_target_pairs={{0,6},{1,59},{2,8},{3,61},{4,10},{5,63},{6,12},{7,1},{8,14},{9,3},... | collective-permute-start | bytes 417800 | tf_op jit(solution)/shard_map/ppermute | solution.py:179
  66.2 8.6 %collective-permute-start.6 = (bf16[32,2176]{1,0:T(8,128)(2,1)S(1)}, bf16[32,2176]{1,0:T(8,128)(2,1)S(1)}, u32[]{:S(2)}, u32[]{:S(2)}) collective-permute-start(bf16[32,2176]{1,0:T(8,128)(2,1)S(1)} %collective-permute-done.5.refs_6_), channel_id=1, source_target_pairs={{0,2},{1,63},{2,4},{3,1},{4,6},{5,3},{6,8},{7,5},{8,10},{9,7},{10,... | collective-permute-start | bytes 417800 | tf_op jit(solution)/shard_map/ppermute | solution.py:179
  68.7 10.5 %collective-permute-start.13 = (bf16[32,2176]{1,0:T(8,128)(2,1)S(1)}, bf16[32,2176]{1,0:T(8,128)(2,1)S(1)}, u32[]{:S(2)}, u32[]{:S(2)}) collective-permute-start(bf16[32,2176]{1,0:T(8,128)(2,1)S(1)} %collective-permute-done.11.refs_12_), channel_id=1, source_target_pairs={{0,4},{1,61},{2,6},{3,63},{4,8},{5,1},{6,10},{7,3},{8,12},{9,5},{1... | collective-permute-start | bytes 417800 | tf_op jit(solution)/shard_map/ppermute | solution.py:179
  87.3 7.5 %collective-permute-start.14 = (bf16[32,2176]{1,0:T(8,128)(2,1)S(1)}, bf16[32,2176]{1,0:T(8,128)(2,1)S(1)}, u32[]{:S(2)}, u32[]{:S(2)}) collective-permute-start(bf16[32,2176]{1,0:T(8,128)(2,1)S(1)} %collective-permute-done.13.refs_14_), channel_id=1, source_target_pairs={{0,2},{1,63},{2,4},{3,1},{4,6},{5,3},{6,8},{7,5},{8,10},{9,7},{10,... | collective-permute-start | bytes 417800 | tf_op jit(solution)/shard_map/ppermute | solution.py:179
  101.8 12.4 %collective-permute-start.31 = (bf16[32,2048]{1,0:T(8,128)(2,1)S(1)}, bf16[32,2048]{1,0:T(8,128)(2,1)S(1)}, u32[]{:S(2)}, u32[]{:S(2)}) collective-permute-start(bf16[32,2048]{1,0:T(8,128)(2,1)S(1)} %node.15), channel_id=1, source_target_pairs={{0,60},{1,5},{2,62},{3,7},{4,0},{5,9},{6,2},{7,11},{8,4},{9,13},{1... | collective-permute-start | bytes 393224 | tf_op jit(solution)/shard_map/ppermute | solution.py:179
  110.5 17.2 %collective-permute-start.28 = (bf16[32,2048]{1,0:T(8,128)(2,1)S(1)}, bf16[32,2048]{1,0:T(8,128)(2,1)S(1)}, u32[]{:S(2)}, u32[]{:S(2)}) collective-permute-start(bf16[32,2048]{1,0:T(8,128)(2,1)S(1)} %node.14), channel_id=1, source_target_pairs={{0,62},{1,3},{2,0},{3,5},{4,2},{5,7},{6,4},{7,9},{8,6},{9,11},{10,... | collective-permute-start | bytes 393224 | tf_op jit(solution)/shard_map/ppermute | solution.py:179
  111.9 15.6 %collective-permute-start.25 = (bf16[32,2048]{1,0:T(8,128)(2,1)S(1)}, bf16[32,2048]{1,0:T(8,128)(2,1)S(1)}, u32[]{:S(2)}, u32[]{:S(2)}) collective-permute-start(bf16[32,2048]{1,0:T(8,128)(2,1)S(1)} %node.12), channel_id=1, source_target_pairs={{0,62},{1,3},{2,0},{3,5},{4,2},{5,7},{6,4},{7,9},{8,6},{9,11},{10,... | collective-permute-start | bytes 393224 | tf_op jit(solution)/shard_map/ppermute | solution.py:179
  114.3 13.5 %collective-permute-start.32 = (bf16[32,2048]{1,0:T(8,128)(2,1)S(1)}, bf16[32,2048]{1,0:T(8,128)(2,1)S(1)}, u32[]{:S(2)}, u32[]{:S(2)}) collective-permute-start(bf16[32,2048]{1,0:T(8,128)(2,1)S(1)} %node.16), channel_id=1, source_target_pairs={{0,58},{1,7},{2,60},{3,9},{4,62},{5,11},{6,0},{7,13},{8,2},{9,15},... | collective-permute-start | bytes 393224 | tf_op jit(solution)/shard_map/ppermute | solution.py:179
  124.8 8.4 %collective-permute-start.21 = (bf16[32,2048]{1,0:T(8,128)(2,1)S(1)}, bf16[32,2048]{1,0:T(8,128)(2,1)S(1)}, u32[]{:S(2)}, u32[]{:S(2)}) collective-permute-start(bf16[32,2048]{1,0:T(8,128)(2,1)S(1)} %node.10), channel_id=1, source_target_pairs={{0,62},{1,3},{2,0},{3,5},{4,2},{5,7},{6,4},{7,9},{8,6},{9,11},{10,... | collective-permute-start | bytes 393224 | tf_op jit(solution)/shard_map/ppermute | solution.py:179
  127.6 14.2 %collective-permute-start.26 = (bf16[32,2048]{1,0:T(8,128)(2,1)S(1)}, bf16[32,2048]{1,0:T(8,128)(2,1)S(1)}, u32[]{:S(2)}, u32[]{:S(2)}) collective-permute-start(bf16[32,2048]{1,0:T(8,128)(2,1)S(1)} %node.13), channel_id=1, source_target_pairs={{0,60},{1,5},{2,62},{3,7},{4,0},{5,9},{6,2},{7,11},{8,4},{9,13},{1... | collective-permute-start | bytes 393224 | tf_op jit(solution)/shard_map/ppermute | solution.py:179
  127.9 14.2 %collective-permute-start.33 = (bf16[32,2048]{1,0:T(8,128)(2,1)S(1)}, bf16[32,2048]{1,0:T(8,128)(2,1)S(1)}, u32[]{:S(2)}, u32[]{:S(2)}) collective-permute-start(bf16[32,2048]{1,0:T(8,128)(2,1)S(1)} %node.17), channel_id=1, source_target_pairs={{0,54},{1,11},{2,56},{3,13},{4,58},{5,15},{6,60},{7,17},{8,62},{9,... | collective-permute-start | bytes 393224 | tf_op jit(solution)/shard_map/ppermute | solution.py:179
  131.1 10.7 %collective-permute-start.23 = (bf16[16,2048]{1,0:T(8,128)(2,1)S(1)}, bf16[16,2048]{1,0:T(8,128)(2,1)S(1)}, u32[]{:S(2)}, u32[]{:S(2)}) collective-permute-start(bf16[16,2048]{1,0:T(8,128)(2,1)S(1)} %get-tuple-element.40), channel_id=1, source_target_pairs={{0,62},{1,3},{2,0},{3,5},{4,2},{5,7},{6,4},{7,9},{8,6},{9,11},{10,... | collective-permute-start | bytes 196616 | tf_op jit(solution)/shard_map/ppermute | solution.py:179
  133.3 19.7 %collective-permute-start.22 = (bf16[32,2048]{1,0:T(8,128)(2,1)S(1)}, bf16[32,2048]{1,0:T(8,128)(2,1)S(1)}, u32[]{:S(2)}, u32[]{:S(2)}) collective-permute-start(bf16[32,2048]{1,0:T(8,128)(2,1)S(1)} %node.11), channel_id=1, source_target_pairs={{0,60},{1,5},{2,62},{3,7},{4,0},{5,9},{6,2},{7,11},{8,4},{9,13},{1... | collective-permute-start | bytes 393224 | tf_op jit(solution)/shard_map/ppermute | solution.py:179
  142.2 13.0 %collective-permute-start.34 = (bf16[32,2048]{1,0:T(8,128)(2,1)S(1)}, bf16[32,2048]{1,0:T(8,128)(2,1)S(1)}, u32[]{:S(2)}, u32[]{:S(2)}) collective-permute-start(bf16[32,2048]{1,0:T(8,128)(2,1)S(1)} %node.18), channel_id=1, source_target_pairs={{0,54},{1,11},{2,56},{3,13},{4,58},{5,15},{6,60},{7,17},{8,62},{9,... | collective-permute-start | bytes 393224 | tf_op jit(solution)/shard_map/ppermute | solution.py:179
  (17 other events, 127.1 us)
